TPU v7x, 256 devices: a whole 4x4x8 slice. The times are simulated.
256 devices in a mesh: sp: 64 (over z, x, core), tp: 4 (over y).
Axes of the slice: x: 4, y: 4, z: 8, core: 2. Of those that a mesh axis runs over, the one named last changes fastest.
Arguments:
- queries: bfloat16 [32768, 1024], P('sp', 'tp'), may hold values from -100 to 100
- keys: bfloat16 [32768, 256], P('sp', 'tp'), may hold values from -100 to 100
- values: bfloat16 [32768, 256], P('sp', 'tp'), may hold values from -6 to 6
- sink_logits: float32 [16], P('tp'), may hold values from 2 to 6
- stream: bfloat16 [32768, 2048], P(('sp', 'tp')), may hold values from -6 to 6
- out_proj: bfloat16 [1024, 2048], P('tp'), may hold values from -0.1875 to 0.1875
- norm_gain: float32 [2048], replicated, may hold values from 0.1 to 1.9
- routes: int32 [32768, 2], P(('sp', 'tp')), may hold values from 0 to 63, all different within a row; in each aligned block of 128 rows (0 to 127, 128 to 255, ...) at most 5 rows name the same one
- route_weights: float32 [32768, 2], P(('sp', 'tp')), may hold values from 0.2 to 1
- gate_proj: bfloat16 [64, 2048, 3584], P('sp', None, 'tp'), may hold values from -0.125 to 0.125
- up_proj: bfloat16 [64, 2048, 3584], P('sp', None, 'tp'), may hold values from -0.125 to 0.125
- down_proj: bfloat16 [64, 3584, 2048], P('sp', 'tp'), may hold values from -0.09375 to 0.09375
Outputs:
- layer_out: bfloat16 [32768, 2048], P(('sp', 'tp'))
Inputs may be any that keep to these rules, and one draw needn't show every extreme that they name: `routes`: each row names two different experts. Among the rows of one device after the attention (aligned blocks of 128 rows) no expert is named more than 5 times.
All inputs are finite; a program needn't handle non-finite values.
Results may differ from a plain program's by a relative error of at most 0.009.
Values may be sent and summed in bfloat16 or wider, within the bound.
No kernel may reach another device: no remote copies, remote signals or barrier semaphores. Data moves between devices by JAX's collectives and lax.ppermute only.
A program may use at most 128 MiB of HBM per device.

v0:
```python
import functools
import jax
import jax.numpy as jnp
from jax import lax
from jax.experimental import pallas as pl
from jax.experimental.pallas import tpu as pltpu
from jax.sharding import PartitionSpec as P


DH = 64
WINDOW = 128
EPSILON = 1e-06
CHUNKS = (5,)

F32 = jnp.float32
BF16 = jnp.bfloat16


def around(value, by):
    n = lax.axis_size("tp")
    return lax.ppermute(value, "tp", [(i, (i + by) % n) for i in range(n)])


def partner(value):
    n = lax.axis_size("sp")
    return lax.ppermute(value, "sp", [(i, i ^ 1) for i in range(n)])


def dot(a, b):
    return jnp.dot(a, b, preferred_element_type=F32)


def call(body, outs, scratch=(), mib=16, **kw):
    return pl.pallas_call(
        body,
        out_shape=outs,
        scratch_shapes=list(scratch),
        compiler_params=pltpu.CompilerParams(vmem_limit_bytes=mib << 20),
        **kw,
    )


def route_body(cap, routes_ref, w_ref, pick_ref, pick0_ref, pick1_ref, wcol_ref):
    rows = routes_ref.shape[1]
    experts = pick_ref.shape[0] // cap
    ids = lax.broadcasted_iota(jnp.int32, (experts, rows), 0)
    before = (
        lax.broadcasted_iota(jnp.int32, (rows, rows), 0)
        < lax.broadcasted_iota(jnp.int32, (rows, rows), 1)
    ).astype(F32).astype(BF16)
    hit0 = (ids == routes_ref[0:1, :]).astype(F32)
    hit1 = (ids == routes_ref[1:2, :]).astype(F32)
    rank0 = dot(hit0.astype(BF16), before)
    rank1 = dot(hit1.astype(BF16), before) + jnp.sum(hit0, axis=1, keepdims=True)
    for r in range(cap):
        at0 = jnp.where(rank0 == float(r), hit0, 0.0)
        at1 = jnp.where(rank1 == float(r), hit1, 0.0)
        here = slice(r * experts, (r + 1) * experts)
        pick0_ref[here, :] = at0.astype(BF16)
        pick1_ref[here, :] = at1.astype(BF16)
        pick_ref[here, :] = (at0 + at1).astype(BF16)
    for k in range(2):
        spread = jnp.broadcast_to(w_ref[k : k + 1, :], (rows, rows))
        wcol_ref[:, k * rows : (k + 1) * rows] = spread.T


def attend_body(me_ref, first_ref, sink_ref, q_ref, k_ref, v_ref, tail_ref, *refs):
    outs, (band_k, band_v) = refs[:4], refs[4:]
    w = WINDOW
    band_k[0:DH, 0:w] = tail_ref[0:DH, :]
    band_v[0:DH, 0:w] = tail_ref[DH : 2 * DH, :]
    band_k[0:DH, w:] = k_ref[...]
    band_v[0:DH, w:] = v_ref[...]
    qpos = lax.broadcasted_iota(jnp.int32, (2 * w, 2 * w), 0) % w
    kpos = lax.broadcasted_iota(jnp.int32, (2 * w, 2 * w), 1)
    near = (kpos > qpos) & (kpos <= qpos + w)
    lower = lax.broadcasted_iota(jnp.int32, (2 * w, 1), 0) < w
    zero = jnp.zeros((DH, 2 * w), BF16)
    for i in range(4):
        n = lax.rem(me_ref[0] + i, 4)
        at = pl.multiple_of(n * w, w)
        kb = band_k[0:DH, pl.ds(at, 2 * w)]
        vb = band_v[0:DH, pl.ds(at, 2 * w)]
        hidden = jnp.where((first_ref[0] == 1) & (n == 0), w, 0)
        allowed = near & (kpos >= hidden)
        qb = q_ref[pl.ds(at, w), :]
        q2 = jnp.concatenate([qb[:, 0:w], qb[:, w:]], axis=0)
        total = None
        for h in range(2):
            kz = jnp.concatenate([kb, zero] if h == 0 else [zero, kb], axis=0)
            vz = jnp.concatenate([vb, zero] if h == 0 else [zero, vb], axis=0)
            s = dot(q2, kz) * DH ** (-0.5)
            s = jnp.where(allowed, s, -jnp.inf)
            sink = jnp.where(lower, sink_ref[h], sink_ref[2 + h])
            top = jnp.maximum(jnp.max(s, axis=1, keepdims=True), sink)
            e = jnp.exp(s - top)
            den = jnp.sum(e, axis=1, keepdims=True) + jnp.exp(sink - top)
            p = (e / den).astype(BF16)
            o = lax.dot_general(p, vz, (((1,), (1,)), ((), ())), preferred_element_type=F32)
            total = o if total is None else total + o
        outs[i][...] = jnp.concatenate([total[0:w], total[w:]], axis=1).astype(BF16)


def pack_rows(stage, rows, slot, first):
    count = rows.shape[0]
    for s in range(8):
        for k in range(2):
            at = s * 256 + k * 128
            stage[2 * slot + k, pl.ds(first + s, count, stride=8), :] = rows[:, at : at + 128]


def unpack_rows(stage, slot, first, out_ref, at, count):
    for s in range(8):
        for k in range(2):
            got = stage[2 * slot + k, pl.ds(first + s, count, stride=8), :]
            lane = s * 256 + k * 128
            out_ref[at : at + count, lane : lane + 128] = got.astype(BF16)


def load_stage(stage, ref, n):
    for k in range(2 * n):
        stage[k, 0 : ref.shape[0], :] = ref[:, k * 128 : (k + 1) * 128].astype(F32)


def store_stage(out_ref, stage, n):
    for k in range(2 * n):
        out_ref[:, k * 128 : (k + 1) * 128] = stage[k].astype(BF16)


def project_body(cap, half_ref, p_ref, m_ref, a_ref, b_ref, ps_ref, ms_ref, as_ref, bs_ref,
                 h0_ref, h1_ref, h2_ref, h3_ref, own_hbm, stream_hbm, gain_hbm, pick_hbm, mixed_hbm, *refs):
    outs, (stage, own_ref, stream_ref, gain_ref, pick_ref, mixed_ref, sems) = refs[:-7], refs[-7:]
    fetched = [
        pltpu.make_async_copy(src, dst, sems.at[i])
        for i, (src, dst) in enumerate(
            ((own_hbm, own_ref), (stream_hbm, stream_ref), (gain_hbm, gain_ref), (pick_hbm, pick_ref))
        )
    ]
    for copy in fetched:
        copy.start()
    h0, h1, h2, h3 = h0_ref[...], h1_ref[...], h2_ref[...], h3_ref[...]
    mid = a_ref.shape[0]
    wide = own_ref.shape[1] // 2
    for mine, (p, m, a, b) in enumerate(((ps_ref, ms_ref, as_ref, bs_ref), (p_ref, m_ref, a_ref, b_ref))):
        half = half_ref[0] if mine else 1 - half_ref[0]
        here = pl.ds(pl.multiple_of(half * wide, wide), wide)
        part = dot(h1, p[...]) + dot(h3, m[...])
        mixed_ref[:, here] = part + dot(h2[:, :mid], a[...]) + dot(h2[:, mid:], b[...])
    for copy in fetched:
        copy.wait()
    mixed = mixed_ref[...] + dot(h0, own_ref[...]) + stream_ref[...].astype(F32)
    mixed_ref[...] = mixed
    kept = pltpu.make_async_copy(mixed_ref, mixed_hbm, sems.at[4])
    kept.start()
    scale = lax.rsqrt(jnp.mean(mixed * mixed, axis=1, keepdims=True) + EPSILON)
    normed = (mixed * scale * gain_ref[...]).astype(BF16)
    experts = pick_ref.shape[0] // cap
    slot = 0
    for c, n in enumerate(CHUNKS):
        for r in range(n):
            rows = dot(pick_ref[slot * experts : (slot + 1) * experts, :], normed)
            pack_rows(stage, rows, r, 0)
            slot += 1
        store_stage(outs[c], stage, n)
    kept.wait()


def expert_body(n, ins, *refs):
    blocks, (gate_ref, up_ref, down_ref) = refs[:ins], refs[ins : ins + 3]
    outs, (stage, x, act, gates, ups, downs, sems) = refs[ins + 3 : -7], refs[-7:]
    h = outs[0].shape[0]
    srcs = h // n
    cols = act.shape[2]

    def fetch(i):
        here = pl.ds(pl.multiple_of(i * cols, cols), cols)
        return (
            pltpu.make_async_copy(gate_ref.at[0, :, here], gates.at[i], sems.at[0, i]),
            pltpu.make_async_copy(up_ref.at[0, :, here], ups.at[i], sems.at[1, i]),
        )

    def fetch_down():
        return pltpu.make_async_copy(down_ref.at[0], downs, sems.at[2, 0])

    for i in range(act.shape[0]):
        for copy in fetch(i):
            copy.start()
    fetch_down().start()
    row = 0
    for ref in blocks:
        load_stage(stage, ref, n)
        for half in range(ref.shape[0] // (8 * srcs)):
            for r in range(n):
                unpack_rows(stage, r, half * 8 * srcs, x, row, srcs)
                row += srcs

    def hidden_tile(i, carry):
        for copy in fetch(i):
            copy.wait()
        both = jnp.concatenate([gates[i], ups[i]], axis=1)
        gu = dot(x[...], both)
        g, u = gu[:, :cols], gu[:, cols:]
        act[i] = (g * (1.0 / (1.0 + jnp.exp(-g))) * u).astype(BF16)
        return carry

    lax.fori_loop(0, act.shape[0], hidden_tile, 0)
    fetch_down().wait()
    hid = jnp.concatenate([act[i] for i in range(act.shape[0])], axis=1)
    wide = 256

    def out_tile(t, carry):
        here = pl.ds(pl.multiple_of(t * wide, wide), wide)
        y = dot(hid, downs[:, here]).astype(BF16)
        for k, out in enumerate(outs):
            out[:, here] = y[k * h : (k + 1) * h]
        return carry

    lax.fori_loop(0, downs.shape[1] // wide, out_tile, 0)


def gathered_body(n, own_top, own_bottom, plus_ref, minus_ref, fromleft_ref, fromright_ref, out_ref, stage):
    h = fromleft_ref.shape[0]
    srcs = h // n
    top = own_top[...].astype(F32) + minus_ref[...].astype(F32) + fromleft_ref[...].astype(F32)
    bottom = own_bottom[...].astype(F32) + plus_ref[...].astype(F32) + fromright_ref[...].astype(F32)
    for half, rows in enumerate((top, bottom)):
        for r in range(n):
            pack_rows(stage, rows[r * srcs : (r + 1) * srcs], r, half * 8 * srcs)
    store_stage(out_ref, stage, n)


def combine_body(cap, *refs):
    rets, refs = refs[: len(CHUNKS)], refs[len(CHUNKS) :]
    pick0_hbm, pick1_hbm, wcol_hbm, mixed_hbm, out_ref, stage, back = refs[:7]
    pick0_ref, pick1_ref, wcol_ref, mixed_ref, sems = refs[7:]
    fetched = [
        pltpu.make_async_copy(src, dst, sems.at[i])
        for i, (src, dst) in enumerate(
            ((pick0_hbm, pick0_ref), (pick1_hbm, pick1_ref), (wcol_hbm, wcol_ref), (mixed_hbm, mixed_ref))
        )
    ]
    for copy in fetched:
        copy.start()
    experts = pick0_ref.shape[0] // cap
    slot = 0
    for ref, n in zip(rets, CHUNKS):
        load_stage(stage, ref, n)
        for r in range(n):
            unpack_rows(stage, r, 0, back, slot * experts, experts)
            slot += 1
    for copy in fetched:
        copy.wait()
    rows = mixed_ref.shape[0]
    one = (((0,), (0,)), ((), ()))
    for t in range(mixed_ref.shape[1] // 256):
        here = slice(t * 256, (t + 1) * 256)
        o0 = lax.dot_general(pick0_ref[...], back[:, here], one, preferred_element_type=F32)
        o1 = lax.dot_general(pick1_ref[...], back[:, here], one, preferred_element_type=F32)
        for lane in range(0, 256, rows):
            at = slice(t * 256 + lane, t * 256 + lane + rows)
            out_ref[:, at] = (
                mixed_ref[:, at]
                + wcol_ref[:, :rows] * o0[:, lane : lane + rows]
                + wcol_ref[:, rows:] * o1[:, lane : lane + rows]
            ).astype(BF16)


def on_device(queries, keys, values, sink_logits, stream, out_proj, norm_gain, routes, route_weights,
              gate_proj, up_proj, down_proj):
    vmem = pl.BlockSpec(memory_space=pltpu.VMEM)
    smem = pl.BlockSpec(memory_space=pltpu.SMEM)
    tok_sp, width = queries.shape
    rows, d = stream.shape
    experts = lax.axis_size("sp")
    cap = max(2, (5 * rows + 2 * experts - 1) // (2 * experts))
    sp, tp = lax.axis_index("sp"), lax.axis_index("tp")
    key_t, value_t = keys.T, values.T

    tail = jnp.concatenate([key_t[:, tok_sp - WINDOW :], value_t[:, tok_sp - WINDOW :]], axis=0)
    tail = lax.ppermute(tail, "sp", [(i, i + 1) for i in range(experts - 1)])

    core = lax.rem(sp, 2)
    wide = d // 2
    w_own = lax.dynamic_slice(out_proj, (0, core * wide), (width, wide))
    w_p, w_m = around(w_own, 1), around(w_own, -1)

    slots = experts * cap
    pick, pick0, pick1, wcol = call(
        functools.partial(route_body, cap),
        [jax.ShapeDtypeStruct((slots, rows), BF16)] * 3 + [jax.ShapeDtypeStruct((rows, 2 * rows), F32)],
        mib=58,
    )(routes.T, route_weights.T)

    heads = call(
        attend_body,
        [jax.ShapeDtypeStruct((WINDOW, width), BF16)] * 4,
        [pltpu.VMEM((DH, tok_sp + WINDOW), BF16)] * 2,
        in_specs=[smem, smem, smem, vmem, vmem, vmem, vmem],
        mib=58,
    )(tp.reshape(1), (sp == 0).astype(jnp.int32).reshape(1), sink_logits, queries, key_t, value_t, tail)
    heads = [heads[0]] + [around(heads[i], i) for i in (1, 2, 3)]
    w_p, w_m, heads = lax.optimization_barrier((w_p, w_m, heads))
    w_a, w_b = around(w_p[: width // 2], 1), around(w_m[width // 2 :], -1)
    w_ps, w_ms, w_as, w_bs = partner(w_p), partner(w_m), partner(w_a), partner(w_b)

    hbm = pl.BlockSpec(memory_space=pltpu.HBM)
    mixed, *outgoing = call(
        functools.partial(project_body, cap),
        [jax.ShapeDtypeStruct((rows, d), F32)]
        + [jax.ShapeDtypeStruct((experts * 8, 256 * n), BF16) for n in CHUNKS],
        [
            pltpu.VMEM((2 * max(CHUNKS), experts * 8, 128), F32),
            pltpu.VMEM((width, d), BF16),
            pltpu.VMEM((rows, d), BF16),
            pltpu.VMEM((1, d), F32),
            pltpu.VMEM((slots, rows), BF16),
            pltpu.VMEM((rows, d), F32),
            pltpu.SemaphoreType.DMA((5,)),
        ],
        in_specs=[smem] + [vmem] * 12 + [hbm] * 4,
        out_specs=[hbm] + [vmem] * len(CHUNKS),
        mib=20,
    )(core.reshape(1), w_p, w_m, w_a, w_b, w_ps, w_ms, w_as, w_bs, *heads, out_proj, stream,
      norm_gain.reshape(1, d), pick)

    vm = lambda k: [vmem] * k
    cols = 128
    hidden = gate_proj.shape[2]
    n = CHUNKS[0]
    h = experts * n // 2
    add = lambda a, b: (a.astype(F32) + b.astype(F32)).astype(BF16)
    tie = lax.optimization_barrier

    def run_experts(*blocks):
        tall = sum(v.shape[0] for v in blocks) // 8 * n
        return call(
            functools.partial(expert_body, n, len(blocks)),
            [jax.ShapeDtypeStruct((h, d), BF16)] * (tall // h),
            [
                pltpu.VMEM((2 * n, experts * 8, 128), F32),
                pltpu.VMEM((tall, d), BF16),
                pltpu.VMEM((hidden // cols, tall, cols), BF16),
                pltpu.VMEM((hidden // cols, d, cols), BF16),
                pltpu.VMEM((hidden // cols, d, cols), BF16),
                pltpu.VMEM((hidden, d), BF16),
                pltpu.SemaphoreType.DMA((3, hidden // cols)),
            ],
            in_specs=vm(len(blocks)) + [hbm] * 3,
            out_specs=vm(tall // h),
            mib=28,
            cost_estimate=pl.CostEstimate(
                flops=6 * tall * d * hidden, transcendentals=tall * hidden, bytes_accessed=6 * d * hidden
            ),
        )(*blocks, gate_proj, up_proj, down_proj)

    block = outgoing[0].reshape(experts, 8, 256 * n)
    arrived = lax.all_to_all(block, "sp", 0, 0, tiled=True).reshape(experts * 8, 256 * n)
    left, right = around(arrived, 1), around(arrived, -1)
    own_top, own_bottom = run_experts(arrived)
    left, right, own_top = tie((left, right, own_top))
    half = experts * 4
    far_a, far_b = around(left[:half], 1), around(right[half:], -1)
    p_top, p_bottom, m_top, m_bottom = run_experts(left, right)
    plus = around(m_bottom, 1)
    minus = around(p_top, -1)
    far_a, far_b, m_top = tie((far_a, far_b, m_top))
    y_a, y_b = run_experts(far_a, far_b)
    top, bottom = add(m_top, around(y_a, 1)), add(p_bottom, around(y_b, -1))
    from_left, from_right = around(top, 1), around(bottom, -1)
    back = call(
        functools.partial(gathered_body, n),
        jax.ShapeDtypeStruct((experts * 8, 256 * n), BF16),
        [pltpu.VMEM((2 * n, experts * 8, 128), F32)],
        in_specs=vm(6),
        out_specs=vmem,
    )(own_top, own_bottom, plus, minus, from_left, from_right)
    back = lax.all_to_all(back.reshape(experts, 8, 256 * n), "sp", 0, 0, tiled=True)
    returned = [back.reshape(experts * 8, 256 * n)]

    return call(
        functools.partial(combine_body, cap),
        jax.ShapeDtypeStruct((rows, d), BF16),
        [
            pltpu.VMEM((2 * max(CHUNKS), experts * 8, 128), F32),
            pltpu.VMEM((slots, d), BF16),
            pltpu.VMEM((slots, rows), BF16),
            pltpu.VMEM((slots, rows), BF16),
            pltpu.VMEM((rows, 2 * rows), F32),
            pltpu.VMEM((rows, d), F32),
            pltpu.SemaphoreType.DMA((4,)),
        ],
        in_specs=vm(len(CHUNKS)) + [hbm] * 4,
        out_specs=vmem,
        mib=20,
    )(*returned, pick0, pick1, wcol, mixed)


def solution(mesh):
    return jax.shard_map(
        on_device,
        mesh=mesh,
        in_specs=(
            P("sp", "tp"),
            P("sp", "tp"),
            P("sp", "tp"),
            P("tp"),
            P(("sp", "tp"), None),
            P("tp", None),
            P(),
            P(("sp", "tp"), None),
            P(("sp", "tp"), None),
            P("sp", None, "tp"),
            P("sp", None, "tp"),
            P("sp", "tp", None),
        ),
        out_specs=P(("sp", "tp"), None),
        check_vma=False,
    )
```

profile of v0, /device:TPU:2, one launch (start us, length us, event | category | flops | bytes accessed | tf_op | source)
XLA Modules:
  0.0 233.9 jit_solution(18015988321034803535)
XLA Ops:
  6.0 1.9 collective-permute-start.2
  7.9 3.3 %collective-permute-done.2.tail_ref = bf16[128,128]{1,0:T(8,128)(2,1)S(1)} collective-permute-done((bf16[128,128]{1,0:T(8,128)(2,1)S(1)}, bf16[128,128]{1,0:T(8,128)(2,1)S(1)}, u32[]{:S(2)}, u32[]{:S(2)}) %collective-permute-start.2) | collective-permute-done | bytes 32800 | tf_op jit(solution)/shard_map/ppermute | solution.py:280
  11.8 3.0 %shard_map.118 = (bf16[128,256]{1,0:T(8,128)(2,1)}, bf16[128,256]{1,0:T(8,128)(2,1)}, bf16[128,256]{1,0:T(8,128)(2,1)}, bf16[128,256]{1,0:T(8,128)(2,1)}) custom-call(s32[1]{0:T(128)} %bitcast.1.me_ref, s32[1]{0:T(128)} %bitcast.2.first_ref, f32[4]{0:T(128)} %sink_ref.1, bf16[512,256]{1,0:T(8,128)(2,1)} %q_ref.1, bf16[64,512]{1,0:T(8,128)(2,1)} %bitcast.20, ...), custom_call_target="tpu_custom_call" | custom-call | tf_op jit(solution)/shard_map/pallas_call | solution.py:294
  15.1 2.9 %collective-permute-start.4 = (bf16[128,256]{1,0:T(8,128)(2,1)}, bf16[128,256]{1,0:T(8,128)(2,1)S(1)}, u32[]{:S(2)}, u32[]{:S(2)}) collective-permute-start(bf16[128,256]{1,0:T(8,128)(2,1)} %get-tuple-element.37), channel_id=1, source_target_pairs={{0,2},{1,3},{2,0},{3,1},{4,6},{5,7},{6,4},{7,5},{8,10},{9,11},{10,... | collective-permute-start | bytes 196616 | tf_op jit(solution)/shard_map/ppermute | solution.py:21
  23.5 2.4 %collective-permute-start.7 = (bf16[128,1024]{1,0:T(8,128)(2,1)S(1)}, bf16[128,1024]{1,0:T(8,128)(2,1)S(1)}, u32[]{:S(2)}, u32[]{:S(2)}) collective-permute-start(bf16[128,1024]{1,0:T(8,128)(2,1)S(1)} %slice.21), channel_id=1, source_target_pairs={{0,3},{1,0},{2,1},{3,2},{4,7},{5,4},{6,5},{7,6},{8,11},{9,8},{10,9... | collective-permute-start | bytes 786440 | tf_op jit(solution)/shard_map/ppermute | solution.py:21
  26.4 3.7 %collective-permute-done.6.a_ref = bf16[128,1024]{1,0:T(8,128)(2,1)S(1)} collective-permute-done((bf16[128,1024]{1,0:T(8,128)(2,1)S(1)}, bf16[128,1024]{1,0:T(8,128)(2,1)S(1)}, u32[]{:S(2)}, u32[]{:S(2)}) %collective-permute-start.6) | collective-permute-done | bytes 262176 | tf_op jit(solution)/shard_map/ppermute | solution.py:21
  34.1 2.4 %shard_map.120 = (f32[128,2048]{1,0:T(8,128)S(1)}, bf16[512,1280]{1,0:T(8,128)(2,1)S(1)}) custom-call(s32[1]{0:T(128)} %bitcast.half_ref, bf16[256,1024]{1,0:T(8,128)(2,1)S(1)} %collective-permute-done.p_ref, bf16[256,1024]{1,0:T(8,128)(2,1)S(1)} %collective-permute-done.1.m_ref, bf16[128,1024]{1,0:T(8,128)(2,1)S(1)} %collective-permute-done.6.a_ref, ...), custom_call_target="tpu_custom_call" | custom-call | tf_op jit(solution)/shard_map/pallas_call | solution.py:307
  36.4 48.0 %all_to_all.10 = bf16[64,8,1280]{2,1,0:T(8,128)(2,1)S(1)} all-to-all(bf16[64,8,1280]{2,1,0:T(8,128)(2,1)S(1)} %bitcast.14), channel_id=1, replica_groups=mesh['sp'=64,'tp'=4] {'sp'}, dimensions={0} | all-to-all | bytes 2621440 | tf_op jit(solution)/shard_map/all_to_all | solution.py:357
  84.8 2.8 %collective-permute-start.13 = (bf16[512,1280]{1,0:T(8,128)(2,1)S(1)}, bf16[512,1280]{1,0:T(8,128)(2,1)S(1)}, u32[]{:S(2)}, u32[]{:S(2)}) collective-permute-start(bf16[512,1280]{1,0:T(8,128)(2,1)S(1)} %bitcast.16), channel_id=1, source_target_pairs={{0,3},{1,0},{2,1},{3,2},{4,7},{5,4},{6,5},{7,6},{8,11},{9,8},{10,9... | collective-permute-start | bytes 3932168 | tf_op jit(solution)/shard_map/ppermute | solution.py:21
  87.7 2.0 copy-done.10
  89.7 8.8 %shard_map.121 = (bf16[160,2048]{1,0:T(8,128)(2,1)S(1)}, bf16[160,2048]{1,0:T(8,128)(2,1)S(1)}) custom-call(bf16[512,1280]{1,0:T(8,128)(2,1)S(1)} %bitcast.17, bf16[1,2048,896]{2,1,0:T(8,128)(2,1)S(1)} %copy-done.8, bf16[1,2048,896]{2,1,0:T(8,128)(2,1)S(1)} %copy-done.9, bf16[1,896,2048]{2,1,0:T(8,128)(2,1)S(1)} %copy-done.10), custom_call_target="tpu_custom_call" | custom-call | flops 3523215360 | bytes 11010048 | tf_op jit(solution)/shard_map/pallas_call | solution.py:336
  98.5 16.2 %collective-permute-done.12.refs_0_ = bf16[512,1280]{1,0:T(8,128)(2,1)S(1)} collective-permute-done((bf16[512,1280]{1,0:T(8,128)(2,1)S(1)}, bf16[512,1280]{1,0:T(8,128)(2,1)S(1)}, u32[]{:S(2)}, u32[]{:S(2)}) %collective-permute-start.12) | collective-permute-done | bytes 1310752 | tf_op jit(solution)/shard_map/ppermute | solution.py:21
  116.1 2.4 %collective-permute-start.17 = (bf16[256,1280]{1,0:T(8,128)(2,1)S(1)}, bf16[256,1280]{1,0:T(8,128)(2,1)S(1)}, u32[]{:S(2)}, u32[]{:S(2)}) collective-permute-start(bf16[256,1280]{1,0:T(8,128)(2,1)S(1)} %slice.23), channel_id=1, source_target_pairs={{0,3},{1,0},{2,1},{3,2},{4,7},{5,4},{6,5},{7,6},{8,11},{9,8},{10,9... | collective-permute-start | bytes 1966088 | tf_op jit(solution)/shard_map/ppermute | solution.py:21
  118.5 13.3 %shard_map.122 = (bf16[160,2048]{1,0:T(8,128)(2,1)S(1)}, bf16[160,2048]{1,0:T(8,128)(2,1)S(1)}, bf16[160,2048]{1,0:T(8,128)(2,1)S(1)}, bf16[160,2048]{1,0:T(8,128)(2,1)S(1)}) custom-call(bf16[512,1280]{1,0:T(8,128)(2,1)S(1)} %collective-permute-done.12.refs_0_, bf16[512,1280]{1,0:T(8,128)(2,1)S(1)} %collective-permute-done.13.refs_1_, ...), custom_call_target="tpu_custom_call" | custom-call | flops 7046430720 | bytes 11010048 | tf_op jit(solution)/shard_map/pallas_call | solution.py:336
  131.8 8.8 %shard_map.123 = (bf16[160,2048]{1,0:T(8,128)(2,1)S(1)}, bf16[160,2048]{1,0:T(8,128)(2,1)S(1)}) custom-call(bf16[256,1280]{1,0:T(8,128)(2,1)S(1)} %collective-permute-done.16.refs_0_, bf16[256,1280]{1,0:T(8,128)(2,1)S(1)} %collective-permute-done.17.refs_1_, bf16[1,2048,896]{2,1,0:T(8,128)(2,1)S(1)} %copy-done.8, bf16[1,2048,896]{2,1,0:T(8,128)(2,1)S(1)} %copy-done.9, ...), custom_call_target="tpu_custom_call" | custom-call | flops 3523215360 | bytes 11010048 | tf_op jit(solution)/shard_map/pallas_call | solution.py:336
  140.6 2.0 collective-permute-start.20
  142.7 3.2 %collective-permute-start.15 = (bf16[160,2048]{1,0:T(8,128)(2,1)S(1)}, bf16[160,2048]{1,0:T(8,128)(2,1)S(1)}, u32[]{:S(2)}, u32[]{:S(2)}) collective-permute-start(bf16[160,2048]{1,0:T(8,128)(2,1)S(1)} %get-tuple-element.53), channel_id=1, source_target_pairs={{0,3},{1,0},{2,1},{3,2},{4,7},{5,4},{6,5},{7,6},{8,11},{9,8},{10,9... | collective-permute-start | bytes 1966088 | tf_op jit(solution)/shard_map/ppermute | solution.py:21
  146.0 12.3 %collective-permute-done.20 = bf16[160,2048]{1,0:T(8,128)(2,1)S(1)} collective-permute-done((bf16[160,2048]{1,0:T(8,128)(2,1)S(1)}, bf16[160,2048]{1,0:T(8,128)(2,1)S(1)}, u32[]{:S(2)}, u32[]{:S(2)}) %collective-permute-start.20) | collective-permute-done | bytes 655392 | tf_op jit(solution)/shard_map/ppermute | solution.py:21
  158.5 3.2 %collective-permute-start.21 = (bf16[160,2048]{1,0:T(8,128)(2,1)S(1)}, bf16[160,2048]{1,0:T(8,128)(2,1)S(1)}, u32[]{:S(2)}, u32[]{:S(2)}) collective-permute-start(bf16[160,2048]{1,0:T(8,128)(2,1)S(1)} %add_convert_fusion), channel_id=1, source_target_pairs={{0,3},{1,0},{2,1},{3,2},{4,7},{5,4},{6,5},{7,6},{8,11},{9,8},{10,9... | collective-permute-start | bytes 1966088 | tf_op jit(solution)/shard_map/ppermute | solution.py:21
  162.2 13.2 %collective-permute-done.14.plus_ref = bf16[160,2048]{1,0:T(8,128)(2,1)S(1)} collective-permute-done((bf16[160,2048]{1,0:T(8,128)(2,1)S(1)}, bf16[160,2048]{1,0:T(8,128)(2,1)S(1)}, u32[]{:S(2)}, u32[]{:S(2)}) %collective-permute-start.14) | collective-permute-done | bytes 655392 | tf_op jit(solution)/shard_map/ppermute | solution.py:21
  175.4 7.0 %collective-permute-done.21.fromright_ref = bf16[160,2048]{1,0:T(8,128)(2,1)S(1)} collective-permute-done((bf16[160,2048]{1,0:T(8,128)(2,1)S(1)}, bf16[160,2048]{1,0:T(8,128)(2,1)S(1)}, u32[]{:S(2)}, u32[]{:S(2)}) %collective-permute-start.21) | collective-permute-done | bytes 655392 | tf_op jit(solution)/shard_map/ppermute | solution.py:21
  182.5 2.4 %collective-permute-done.19.fromleft_ref = bf16[160,2048]{1,0:T(8,128)(2,1)S(1)} collective-permute-done((bf16[160,2048]{1,0:T(8,128)(2,1)S(1)}, bf16[160,2048]{1,0:T(8,128)(2,1)S(1)}, u32[]{:S(2)}, u32[]{:S(2)}) %collective-permute-start.19) | collective-permute-done | bytes 655392 | tf_op jit(solution)/shard_map/ppermute | solution.py:21
  186.1 44.8 %all_to_all.11 = bf16[64,8,1280]{2,1,0:T(8,128)(2,1)S(1)} all-to-all(bf16[64,8,1280]{2,1,0:T(8,128)(2,1)S(1)} %bitcast.12), channel_id=1, replica_groups=mesh['sp'=64,'tp'=4] {'sp'}, dimensions={0} | all-to-all | bytes 2621440 | tf_op jit(solution)/shard_map/all_to_all | solution.py:377
  230.9 2.7 %shard_map.125 = bf16[128,2048]{1,0:T(8,128)(2,1)} custom-call(bf16[512,1280]{1,0:T(8,128)(2,1)S(1)} %bitcast.13, bf16[320,128]{1,0:T(8,128)(2,1)S(1)} %copy-done.3, bf16[320,128]{1,0:T(8,128)(2,1)S(1)} %copy-done.4, f32[128,256]{1,0:T(8,128)S(1)} %copy-done.2, f32[128,2048]{1,0:T(8,128)S(1)} %get-tuple-element.64.refs_4_), custom_call_target="tpu_custom_call" | custom-call | tf_op jit(solution)/shard_map/pallas_call | solution.py:380
  (64 shorter events, 20.5 us)
Async XLA Ops:
  1.2 21.3 %collective-permute-start = (bf16[256,1024]{1,0:T(8,128)(2,1)S(1)}, bf16[256,1024]{1,0:T(8,128)(2,1)S(1)}, u32[]{:S(2)}, u32[]{:S(2)}) collective-permute-start(bf16[256,1024]{1,0:T(8,128)(2,1)S(1)} %constant_dynamic-slice_fusion), channel_id=1, source_target_pairs={{0,1},{1,2},{2,3},{3,0},{4,5},{5,6},{6,7},{7,4},{8,9},{9,10},{10,1... | collective-permute-start | bytes 1572872 | tf_op jit(solution)/shard_map/ppermute | solution.py:21
  2.9 19.6 %collective-permute-start.1 = (bf16[256,1024]{1,0:T(8,128)(2,1)S(1)}, bf16[256,1024]{1,0:T(8,128)(2,1)S(1)}, u32[]{:S(2)}, u32[]{:S(2)}) collective-permute-start(bf16[256,1024]{1,0:T(8,128)(2,1)S(1)} %constant_dynamic-slice_fusion), channel_id=1, source_target_pairs={{0,3},{1,0},{2,1},{3,2},{4,7},{5,4},{6,5},{7,6},{8,11},{9,8},{10,9... | collective-permute-start | bytes 1572872 | tf_op jit(solution)/shard_map/ppermute | solution.py:21
  6.0 5.2 %collective-permute-start.2 = (bf16[128,128]{1,0:T(8,128)(2,1)S(1)}, bf16[128,128]{1,0:T(8,128)(2,1)S(1)}, u32[]{:S(2)}, u32[]{:S(2)}) collective-permute-start(bf16[128,128]{1,0:T(8,128)(2,1)S(1)} %pad_maximum_fusion), channel_id=1, source_target_pairs={{0,4},{4,8},{8,12},{12,16},{16,20},{20,24},{24,28},{28,32},{32,36}... | collective-permute-start | bytes 98312 | tf_op jit(solution)/shard_map/ppermute | solution.py:280
  14.7 5.7 %collective-permute-start.3 = (bf16[128,256]{1,0:T(8,128)(2,1)}, bf16[128,256]{1,0:T(8,128)(2,1)S(1)}, u32[]{:S(2)}, u32[]{:S(2)}) collective-permute-start(bf16[128,256]{1,0:T(8,128)(2,1)} %get-tuple-element.36), channel_id=1, source_target_pairs={{0,1},{1,2},{2,3},{3,0},{4,5},{5,6},{6,7},{7,4},{8,9},{9,10},{10,1... | collective-permute-start | bytes 196616 | tf_op jit(solution)/shard_map/ppermute | solution.py:21
  15.1 6.1 %collective-permute-start.4 = (bf16[128,256]{1,0:T(8,128)(2,1)}, bf16[128,256]{1,0:T(8,128)(2,1)S(1)}, u32[]{:S(2)}, u32[]{:S(2)}) collective-permute-start(bf16[128,256]{1,0:T(8,128)(2,1)} %get-tuple-element.37), channel_id=1, source_target_pairs={{0,2},{1,3},{2,0},{3,1},{4,6},{5,7},{6,4},{7,5},{8,10},{9,11},{10,... | collective-permute-start | bytes 196616 | tf_op jit(solution)/shard_map/ppermute | solution.py:21
  18.0 4.5 %collective-permute-start.5 = (bf16[128,256]{1,0:T(8,128)(2,1)}, bf16[128,256]{1,0:T(8,128)(2,1)S(1)}, u32[]{:S(2)}, u32[]{:S(2)}) collective-permute-start(bf16[128,256]{1,0:T(8,128)(2,1)} %get-tuple-element.38), channel_id=1, source_target_pairs={{0,3},{1,0},{2,1},{3,2},{4,7},{5,4},{6,5},{7,6},{8,11},{9,8},{10,9... | collective-permute-start | bytes 196616 | tf_op jit(solution)/shard_map/ppermute | solution.py:21
  22.5 7.7 %collective-permute-start.6 = (bf16[128,1024]{1,0:T(8,128)(2,1)S(1)}, bf16[128,1024]{1,0:T(8,128)(2,1)S(1)}, u32[]{:S(2)}, u32[]{:S(2)}) collective-permute-start(bf16[128,1024]{1,0:T(8,128)(2,1)S(1)} %slice.20), channel_id=1, source_target_pairs={{0,1},{1,2},{2,3},{3,0},{4,5},{5,6},{6,7},{7,4},{8,9},{9,10},{10,1... | collective-permute-start | bytes 786440 | tf_op jit(solution)/shard_map/ppermute | solution.py:21
  23.5 6.7 %collective-permute-start.7 = (bf16[128,1024]{1,0:T(8,128)(2,1)S(1)}, bf16[128,1024]{1,0:T(8,128)(2,1)S(1)}, u32[]{:S(2)}, u32[]{:S(2)}) collective-permute-start(bf16[128,1024]{1,0:T(8,128)(2,1)S(1)} %slice.21), channel_id=1, source_target_pairs={{0,3},{1,0},{2,1},{3,2},{4,7},{5,4},{6,5},{7,6},{8,11},{9,8},{10,9... | collective-permute-start | bytes 786440 | tf_op jit(solution)/shard_map/ppermute | solution.py:21
  25.9 6.4 %collective-permute-start.8 = (bf16[256,1024]{1,0:T(8,128)(2,1)S(1)}, bf16[256,1024]{1,0:T(8,128)(2,1)S(1)}, u32[]{:S(2)}, u32[]{:S(2)}) collective-permute-start(bf16[256,1024]{1,0:T(8,128)(2,1)S(1)} %collective-permute-done.p_ref), channel_id=1, source_target_pairs={{0,4},{4,0},{8,12},{12,8},{16,20},{20,16},{24,28},{28,24},{32,36},... | collective-permute-start | bytes 1572872 | tf_op jit(solution)/shard_map/ppermute | solution.py:26
  25.9 6.4 %collective-permute-start.9 = (bf16[256,1024]{1,0:T(8,128)(2,1)S(1)}, bf16[256,1024]{1,0:T(8,128)(2,1)S(1)}, u32[]{:S(2)}, u32[]{:S(2)}) collective-permute-start(bf16[256,1024]{1,0:T(8,128)(2,1)S(1)} %collective-permute-done.1.m_ref), channel_id=1, source_target_pairs={{0,4},{4,0},{8,12},{12,8},{16,20},{20,16},{24,28},{28,24},{32,36},... | collective-permute-start | bytes 1572872 | tf_op jit(solution)/shard_map/ppermute | solution.py:26
  30.2 2.1 collective-permute-start.10
  30.2 2.1 collective-permute-start.11
  34.1 53.6 %copy-start.8 = (bf16[1,2048,896]{2,1,0:T(8,128)(2,1)S(1)}, bf16[1,2048,896]{2,1,0:T(8,128)(2,1)}, u32[]{:S(2)}) copy-start(bf16[1,2048,896]{2,1,0:T(8,128)(2,1)} %refs_2_.5) | copy-start | bytes 11010052
  34.1 53.6 %copy-start.9 = (bf16[1,2048,896]{2,1,0:T(8,128)(2,1)S(1)}, bf16[1,2048,896]{2,1,0:T(8,128)(2,1)}, u32[]{:S(2)}) copy-start(bf16[1,2048,896]{2,1,0:T(8,128)(2,1)} %refs_3_.5) | copy-start | bytes 11010052
  84.4 30.4 %collective-permute-start.12 = (bf16[512,1280]{1,0:T(8,128)(2,1)S(1)}, bf16[512,1280]{1,0:T(8,128)(2,1)S(1)}, u32[]{:S(2)}, u32[]{:S(2)}) collective-permute-start(bf16[512,1280]{1,0:T(8,128)(2,1)S(1)} %bitcast.15), channel_id=1, source_target_pairs={{0,1},{1,2},{2,3},{3,0},{4,5},{5,6},{6,7},{7,4},{8,9},{9,10},{10,1... | collective-permute-start | bytes 3932168 | tf_op jit(solution)/shard_map/ppermute | solution.py:21
  84.8 30.0 %collective-permute-start.13 = (bf16[512,1280]{1,0:T(8,128)(2,1)S(1)}, bf16[512,1280]{1,0:T(8,128)(2,1)S(1)}, u32[]{:S(2)}, u32[]{:S(2)}) collective-permute-start(bf16[512,1280]{1,0:T(8,128)(2,1)S(1)} %bitcast.16), channel_id=1, source_target_pairs={{0,3},{1,0},{2,1},{3,2},{4,7},{5,4},{6,5},{7,6},{8,11},{9,8},{10,9... | collective-permute-start | bytes 3932168 | tf_op jit(solution)/shard_map/ppermute | solution.py:21
  114.8 16.9 %collective-permute-start.16 = (bf16[256,1280]{1,0:T(8,128)(2,1)S(1)}, bf16[256,1280]{1,0:T(8,128)(2,1)S(1)}, u32[]{:S(2)}, u32[]{:S(2)}) collective-permute-start(bf16[256,1280]{1,0:T(8,128)(2,1)S(1)} %slice.22), channel_id=1, source_target_pairs={{0,1},{1,2},{2,3},{3,0},{4,5},{5,6},{6,7},{7,4},{8,9},{9,10},{10,1... | collective-permute-start | bytes 1966088 | tf_op jit(solution)/shard_map/ppermute | solution.py:21
  116.1 15.7 %collective-permute-start.17 = (bf16[256,1280]{1,0:T(8,128)(2,1)S(1)}, bf16[256,1280]{1,0:T(8,128)(2,1)S(1)}, u32[]{:S(2)}, u32[]{:S(2)}) collective-permute-start(bf16[256,1280]{1,0:T(8,128)(2,1)S(1)} %slice.23), channel_id=1, source_target_pairs={{0,3},{1,0},{2,1},{3,2},{4,7},{5,4},{6,5},{7,6},{8,11},{9,8},{10,9... | collective-permute-start | bytes 1966088 | tf_op jit(solution)/shard_map/ppermute | solution.py:21
  140.6 17.7 %collective-permute-start.20 = (bf16[160,2048]{1,0:T(8,128)(2,1)S(1)}, bf16[160,2048]{1,0:T(8,128)(2,1)S(1)}, u32[]{:S(2)}, u32[]{:S(2)}) collective-permute-start(bf16[160,2048]{1,0:T(8,128)(2,1)S(1)} %get-tuple-element.60), channel_id=1, source_target_pairs={{0,3},{1,0},{2,1},{3,2},{4,7},{5,4},{6,5},{7,6},{8,11},{9,8},{10,9... | collective-permute-start | bytes 1966088 | tf_op jit(solution)/shard_map/ppermute | solution.py:21
  142.6 19.1 %collective-permute-start.18 = (bf16[160,2048]{1,0:T(8,128)(2,1)S(1)}, bf16[160,2048]{1,0:T(8,128)(2,1)S(1)}, u32[]{:S(2)}, u32[]{:S(2)}) collective-permute-start(bf16[160,2048]{1,0:T(8,128)(2,1)S(1)} %get-tuple-element.58), channel_id=1, source_target_pairs={{0,1},{1,2},{2,3},{3,0},{4,5},{5,6},{6,7},{7,4},{8,9},{9,10},{10,1... | collective-permute-start | bytes 1966088 | tf_op jit(solution)/shard_map/ppermute | solution.py:21
  142.7 32.7 %collective-permute-start.14 = (bf16[160,2048]{1,0:T(8,128)(2,1)S(1)}, bf16[160,2048]{1,0:T(8,128)(2,1)S(1)}, u32[]{:S(2)}, u32[]{:S(2)}) collective-permute-start(bf16[160,2048]{1,0:T(8,128)(2,1)S(1)} %get-tuple-element.52), channel_id=1, source_target_pairs={{0,1},{1,2},{2,3},{3,0},{4,5},{5,6},{6,7},{7,4},{8,9},{9,10},{10,1... | collective-permute-start | bytes 1966088 | tf_op jit(solution)/shard_map/ppermute | solution.py:21
  142.7 32.7 %collective-permute-start.15 = (bf16[160,2048]{1,0:T(8,128)(2,1)S(1)}, bf16[160,2048]{1,0:T(8,128)(2,1)S(1)}, u32[]{:S(2)}, u32[]{:S(2)}) collective-permute-start(bf16[160,2048]{1,0:T(8,128)(2,1)S(1)} %get-tuple-element.53), channel_id=1, source_target_pairs={{0,3},{1,0},{2,1},{3,2},{4,7},{5,4},{6,5},{7,6},{8,11},{9,8},{10,9... | collective-permute-start | bytes 1966088 | tf_op jit(solution)/shard_map/ppermute | solution.py:21
  158.5 24.0 %collective-permute-start.21 = (bf16[160,2048]{1,0:T(8,128)(2,1)S(1)}, bf16[160,2048]{1,0:T(8,128)(2,1)S(1)}, u32[]{:S(2)}, u32[]{:S(2)}) collective-permute-start(bf16[160,2048]{1,0:T(8,128)(2,1)S(1)} %add_convert_fusion), channel_id=1, source_target_pairs={{0,3},{1,0},{2,1},{3,2},{4,7},{5,4},{6,5},{7,6},{8,11},{9,8},{10,9... | collective-permute-start | bytes 1966088 | tf_op jit(solution)/shard_map/ppermute | solution.py:21
  161.9 23.0 %collective-permute-start.19 = (bf16[160,2048]{1,0:T(8,128)(2,1)S(1)}, bf16[160,2048]{1,0:T(8,128)(2,1)S(1)}, u32[]{:S(2)}, u32[]{:S(2)}) collective-permute-start(bf16[160,2048]{1,0:T(8,128)(2,1)S(1)} %add_convert_fusion.1), channel_id=1, source_target_pairs={{0,1},{1,2},{2,3},{3,0},{4,5},{5,6},{6,7},{7,4},{8,9},{9,10},{10,1... | collective-permute-start | bytes 1966088 | tf_op jit(solution)/shard_map/ppermute | solution.py:21
  (10 other events, 235.9 us)
where the time goes:
time: 235 us; the launch traced here: 234 us
  blocking collectives  92.8 us (39%)
  waiting for transfers between devices  61.4 us (26%)
  Pallas kernels  41.7 us (18%)
  starting transfers between devices  29.9 us (13%)
  local copies, waits for them, and re-layouts  7.15 us (3%)
    ppermute x17, waiting for transfers between devices, around(): return lax.ppermute(value, 'tp', [(i, (i + by) % n) for i in range(n)])  58.1 us
    all_to_all x1, blocking collectives, on_device(): lax.all_to_all(block, 'sp', 0, 0, tiled=True).reshape(experts * 8, 256 * n)  48 us
    all_to_all x1, blocking collectives, on_device(): lax.all_to_all(back.reshape(experts, 8, 256 * n), 'sp', 0, 0, tiled=True)  44.8 us
    pallas_call x3, Pallas kernels, run_experts(): call(functools.partial(expert_body, n, len(blocks)), [jax.ShapeDtypeStruc...  30.9 us
    ppermute x17, starting transfers between devices, around(): return lax.ppermute(value, 'tp', [(i, (i + by) % n) for i in range(n)])  27 us
  transfers between devices with their start and end apart: 22, of which 10 were waited for; matrix products, arithmetic and copies ran while one was open for 1% of the time, Pallas kernels for 11%

commit v1 on v0

--- a/solution.py
+++ b/solution.py
@@ -40,7 +40,20 @@
     )
 
 
-def route_body(cap, routes_ref, w_ref, pick_ref, pick0_ref, pick1_ref, wcol_ref):
+def fetch_all(pairs, sems):
+    copies = [pltpu.make_async_copy(src, dst, sems.at[i]) for i, (src, dst) in enumerate(pairs)]
+    for copy in copies:
+        copy.start()
+    return copies
+
+
+def wait_all(copies):
+    for copy in copies:
+        copy.wait()
+
+
+def route_body(cap, routes_hbm, w_hbm, pick_ref, pick0_ref, pick1_ref, wcol_ref, routes_ref, w_ref, sems):
+    wait_all(fetch_all(((routes_hbm, routes_ref), (w_hbm, w_ref)), sems))
     rows = routes_ref.shape[1]
     experts = pick_ref.shape[0] // cap
     ids = lax.broadcasted_iota(jnp.int32, (experts, rows), 0)
@@ -64,11 +77,13 @@
         wcol_ref[:, k * rows : (k + 1) * rows] = spread.T
 
 
-def attend_body(me_ref, first_ref, sink_ref, q_ref, k_ref, v_ref, tail_ref, *refs):
-    outs, (band_k, band_v) = refs[:4], refs[4:]
+def attend_body(me_ref, first_ref, sink_ref, q_hbm, k_hbm, v_hbm, tail_ref, *refs):
+    outs, (band_k, band_v, q_ref, k_ref, v_ref, sems) = refs[:4], refs[4:]
+    copies = fetch_all(((q_hbm, q_ref), (k_hbm, k_ref), (v_hbm, v_ref)), sems)
     w = WINDOW
     band_k[0:DH, 0:w] = tail_ref[0:DH, :]
     band_v[0:DH, 0:w] = tail_ref[DH : 2 * DH, :]
+    wait_all(copies)
     band_k[0:DH, w:] = k_ref[...]
     band_v[0:DH, w:] = v_ref[...]
     qpos = lax.broadcasted_iota(jnp.int32, (2 * w, 2 * w), 0) % w
@@ -114,7 +129,7 @@
         for k in range(2):
             got = stage[2 * slot + k, pl.ds(first + s, count, stride=8), :]
             lane = s * 256 + k * 128
-            out_ref[at : at + count, lane : lane + 128] = got.astype(BF16)
+            out_ref[pl.ds(at, count), lane : lane + 128] = got.astype(BF16)
 
 
 def load_stage(stage, ref, n):
@@ -127,27 +142,25 @@
         out_ref[:, k * 128 : (k + 1) * 128] = stage[k].astype(BF16)
 
 
-def project_body(cap, half_ref, p_ref, m_ref, a_ref, b_ref, ps_ref, ms_ref, as_ref, bs_ref,
-                 h0_ref, h1_ref, h2_ref, h3_ref, own_hbm, stream_hbm, gain_hbm, pick_hbm, mixed_hbm, *refs):
-    outs, (stage, own_ref, stream_ref, gain_ref, pick_ref, mixed_ref, sems) = refs[:-7], refs[-7:]
-    fetched = [
-        pltpu.make_async_copy(src, dst, sems.at[i])
-        for i, (src, dst) in enumerate(
-            ((own_hbm, own_ref), (stream_hbm, stream_ref), (gain_hbm, gain_ref), (pick_hbm, pick_ref))
-        )
-    ]
-    for copy in fetched:
-        copy.start()
+def project_body(cap, half_ref, *refs):
+    mine, theirs, (h0_ref, h1_ref, h2_ref, h3_ref), refs = refs[:6], refs[6:12], refs[12:16], refs[16:]
+    own_hbm, stream_hbm, gain_hbm, pick_hbm, mixed_hbm = refs[:5]
+    outs, (stage, own_ref, stream_ref, gain_ref, pick_ref, mixed_ref, sems) = refs[5:-7], refs[-7:]
+    fetched = fetch_all(
+        ((own_hbm, own_ref), (stream_hbm, stream_ref), (gain_hbm, gain_ref), (pick_hbm, pick_ref)), sems
+    )
     h0, h1, h2, h3 = h0_ref[...], h1_ref[...], h2_ref[...], h3_ref[...]
-    mid = a_ref.shape[0]
+    mid = mine[0].shape[0]
     wide = own_ref.shape[1] // 2
-    for mine, (p, m, a, b) in enumerate(((ps_ref, ms_ref, as_ref, bs_ref), (p_ref, m_ref, a_ref, b_ref))):
-        half = half_ref[0] if mine else 1 - half_ref[0]
+    sides = [x for h in (h1, h3, h2) for x in (h[:, :mid], h[:, mid:])]
+    for half, parts in ((half_ref[0], mine), (1 - half_ref[0], theirs)):
         here = pl.ds(pl.multiple_of(half * wide, wide), wide)
-        part = dot(h1, p[...]) + dot(h3, m[...])
-        mixed_ref[:, here] = part + dot(h2[:, :mid], a[...]) + dot(h2[:, mid:], b[...])
-    for copy in fetched:
-        copy.wait()
+        part = None
+        for side, w in zip(sides, parts):
+            one = dot(side, w[...])
+            part = one if part is None else part + one
+        mixed_ref[:, here] = part
+    wait_all(fetched)
     mixed = mixed_ref[...] + dot(h0, own_ref[...]) + stream_ref[...].astype(F32)
     mixed_ref[...] = mixed
     kept = pltpu.make_async_copy(mixed_ref, mixed_hbm, sems.at[4])
@@ -190,9 +203,14 @@
     for ref in blocks:
         load_stage(stage, ref, n)
         for half in range(ref.shape[0] // (8 * srcs)):
-            for r in range(n):
-                unpack_rows(stage, r, half * 8 * srcs, x, row, srcs)
-                row += srcs
+            first = row
+
+            def one_slot(r, carry):
+                unpack_rows(stage, r, half * 8 * srcs, x, pl.multiple_of(first + r * srcs, srcs), srcs)
+                return carry
+
+            lax.fori_loop(0, n, one_slot, 0)
+            row += h
 
     def hidden_tile(i, carry):
         for copy in fetch(i):
@@ -233,14 +251,9 @@
     rets, refs = refs[: len(CHUNKS)], refs[len(CHUNKS) :]
     pick0_hbm, pick1_hbm, wcol_hbm, mixed_hbm, out_ref, stage, back = refs[:7]
     pick0_ref, pick1_ref, wcol_ref, mixed_ref, sems = refs[7:]
-    fetched = [
-        pltpu.make_async_copy(src, dst, sems.at[i])
-        for i, (src, dst) in enumerate(
-            ((pick0_hbm, pick0_ref), (pick1_hbm, pick1_ref), (wcol_hbm, wcol_ref), (mixed_hbm, mixed_ref))
-        )
-    ]
-    for copy in fetched:
-        copy.start()
+    fetched = fetch_all(
+        ((pick0_hbm, pick0_ref), (pick1_hbm, pick1_ref), (wcol_hbm, wcol_ref), (mixed_hbm, mixed_ref)), sems
+    )
     experts = pick0_ref.shape[0] // cap
     slot = 0
     for ref, n in zip(rets, CHUNKS):
@@ -248,8 +261,7 @@
         for r in range(n):
             unpack_rows(stage, r, 0, back, slot * experts, experts)
             slot += 1
-    for copy in fetched:
-        copy.wait()
+    wait_all(fetched)
     rows = mixed_ref.shape[0]
     one = (((0,), (0,)), ((), ()))
     for t in range(mixed_ref.shape[1] // 256):
@@ -265,10 +277,17 @@
             ).astype(BF16)
 
 
+def hop(up, down):
+    up = around(up, 1)
+    down = around(down, -1)
+    return up, down
+
+
 def on_device(queries, keys, values, sink_logits, stream, out_proj, norm_gain, routes, route_weights,
               gate_proj, up_proj, down_proj):
     vmem = pl.BlockSpec(memory_space=pltpu.VMEM)
     smem = pl.BlockSpec(memory_space=pltpu.SMEM)
+    hbm = pl.BlockSpec(memory_space=pltpu.HBM)
     tok_sp, width = queries.shape
     rows, d = stream.shape
     experts = lax.axis_size("sp")
@@ -281,29 +300,44 @@
 
     core = lax.rem(sp, 2)
     wide = d // 2
-    w_own = lax.dynamic_slice(out_proj, (0, core * wide), (width, wide))
-    w_p, w_m = around(w_own, 1), around(w_own, -1)
+    mid = width // 2
+    w_top = lax.dynamic_slice(out_proj, (0, core * wide), (mid, wide))
+    w_bottom = lax.dynamic_slice(out_proj, (mid, core * wide), (mid, wide))
+    left_top, right_bottom = hop(w_top, w_bottom)
+    left_bottom, right_top = hop(w_bottom, w_top)
+    far_top, far_bottom = hop(left_top, right_bottom)
+    gathered_w = [left_top, left_bottom, right_top, right_bottom, far_top, far_bottom]
+    for k in range(6):
+        gathered_w.append(partner(gathered_w[k]))
 
     slots = experts * cap
     pick, pick0, pick1, wcol = call(
         functools.partial(route_body, cap),
         [jax.ShapeDtypeStruct((slots, rows), BF16)] * 3 + [jax.ShapeDtypeStruct((rows, 2 * rows), F32)],
-        mib=58,
+        [pltpu.VMEM((2, rows), jnp.int32), pltpu.VMEM((2, rows), F32), pltpu.SemaphoreType.DMA((2,))],
+        in_specs=[hbm] * 2,
+        out_specs=[vmem] * 4,
+        mib=8,
     )(routes.T, route_weights.T)
 
     heads = call(
         attend_body,
         [jax.ShapeDtypeStruct((WINDOW, width), BF16)] * 4,
-        [pltpu.VMEM((DH, tok_sp + WINDOW), BF16)] * 2,
-        in_specs=[smem, smem, smem, vmem, vmem, vmem, vmem],
+        [pltpu.VMEM((DH, tok_sp + WINDOW), BF16)] * 2
+        + [
+            pltpu.VMEM((tok_sp, width), BF16),
+            pltpu.VMEM((DH, tok_sp), BF16),
+            pltpu.VMEM((DH, tok_sp), BF16),
+            pltpu.SemaphoreType.DMA((3,)),
+        ],
+        in_specs=[smem, smem, smem, hbm, hbm, hbm, vmem],
+        out_specs=[vmem] * 4,
         mib=58,
     )(tp.reshape(1), (sp == 0).astype(jnp.int32).reshape(1), sink_logits, queries, key_t, value_t, tail)
-    heads = [heads[0]] + [around(heads[i], i) for i in (1, 2, 3)]
-    w_p, w_m, heads = lax.optimization_barrier((w_p, w_m, heads))
-    w_a, w_b = around(w_p[: width // 2], 1), around(w_m[width // 2 :], -1)
-    w_ps, w_ms, w_as, w_bs = partner(w_p), partner(w_m), partner(w_a), partner(w_b)
-
-    hbm = pl.BlockSpec(memory_space=pltpu.HBM)
+    heads = list(heads)
+    for i in (1, 2, 3):
+        heads[i] = around(heads[i], i)
+
     mixed, *outgoing = call(
         functools.partial(project_body, cap),
         [jax.ShapeDtypeStruct((rows, d), F32)]
@@ -317,10 +351,10 @@
             pltpu.VMEM((rows, d), F32),
             pltpu.SemaphoreType.DMA((5,)),
         ],
-        in_specs=[smem] + [vmem] * 12 + [hbm] * 4,
+        in_specs=[smem] + [vmem] * 16 + [hbm] * 4,
         out_specs=[hbm] + [vmem] * len(CHUNKS),
         mib=20,
-    )(core.reshape(1), w_p, w_m, w_a, w_b, w_ps, w_ms, w_as, w_bs, *heads, out_proj, stream,
+    )(core.reshape(1), *gathered_w, *heads, out_proj, stream,
       norm_gain.reshape(1, d), pick)
 
     vm = lambda k: [vmem] * k
@@ -355,15 +389,16 @@
 
     block = outgoing[0].reshape(experts, 8, 256 * n)
     arrived = lax.all_to_all(block, "sp", 0, 0, tiled=True).reshape(experts * 8, 256 * n)
-    left, right = around(arrived, 1), around(arrived, -1)
+    half = experts * 4
+    top, bottom = arrived[:half], arrived[half:]
+    left_top, right_bottom = hop(top, bottom)
+    left_bottom, right_top = hop(bottom, top)
     own_top, own_bottom = run_experts(arrived)
-    left, right, own_top = tie((left, right, own_top))
-    half = experts * 4
-    far_a, far_b = around(left[:half], 1), around(right[half:], -1)
-    p_top, p_bottom, m_top, m_bottom = run_experts(left, right)
+    left_top, right_bottom, own_top = tie((left_top, right_bottom, own_top))
+    far_a, far_b = hop(left_top, right_bottom)
+    p_top, p_bottom, m_top, m_bottom = run_experts(left_top, left_bottom, right_top, right_bottom)
     plus = around(m_bottom, 1)
     minus = around(p_top, -1)
-    far_a, far_b, m_top = tie((far_a, far_b, m_top))
     y_a, y_b = run_experts(far_a, far_b)
     top, bottom = add(m_top, around(y_a, 1)), add(p_bottom, around(y_b, -1))
     from_left, from_right = around(top, 1), around(bottom, -1)

time: 235 us -> 224 us (0.953)
  waiting for transfers between devices: 61.4 us -> 46.8 us
  starting transfers between devices: 29.9 us -> 37.1 us
    ppermute x17 -> x21, waiting for transfers between devices: 58.1 us -> 42.3 us  [around(): return lax.ppermute(value, 'tp', [(i, (i + by) % n) for i in range(n)])]
    ppermute x17 -> x21, starting transfers between devices: 27 us -> 34 us  [around(): return lax.ppermute(value, 'tp', [(i, (i + by) % n) for i in range(n)])]
  transfers between devices with their start and end apart: 22 -> 28, of which waited for: 10 -> 14; matrix products, arithmetic and copies ran while one was open for 1% -> 1% of each run, Pallas kernels for 11% -> 16%
where the time goes in v1:
time: 224 us
  blocking collectives  91.2 us (41%)
  waiting for transfers between devices  46.8 us (21%)
  Pallas kernels  41.5 us (19%)
  starting transfers between devices  37.1 us (17%)
  local copies, waits for them, and re-layouts  6.21 us (3%)
    all_to_all x1, blocking collectives, on_device(): lax.all_to_all(block, 'sp', 0, 0, tiled=True).reshape(experts * 8, 256 * n)  46.3 us
    all_to_all x1, blocking collectives, on_device(): lax.all_to_all(back.reshape(experts, 8, 256 * n), 'sp', 0, 0, tiled=True)  44.9 us
    ppermute x21, waiting for transfers between devices, around(): return lax.ppermute(value, 'tp', [(i, (i + by) % n) for i in range(n)])  42.3 us
    ppermute x21, starting transfers between devices, around(): return lax.ppermute(value, 'tp', [(i, (i + by) % n) for i in range(n)])  34 us
    pallas_call x3, Pallas kernels, run_experts(): call(functools.partial(expert_body, n, len(blocks)), [jax.ShapeDtypeStruc...  31.1 us
  transfers between devices with their start and end apart: 28, of which 14 were waited for; matrix products, arithmetic and copies ran while one was open for 1% of the time, Pallas kernels for 16%

profile of v1, /device:TPU:2, one launch (start us, length us, event | category | flops | bytes accessed | tf_op | source)
XLA Modules:
  0.0 223.6 jit_solution(14276707629319686431)
XLA Ops:
  6.0 1.9 collective-permute-start.12
  7.9 3.3 %collective-permute-done.12.tail_ref = bf16[128,128]{1,0:T(8,128)(2,1)S(1)} collective-permute-done((bf16[128,128]{1,0:T(8,128)(2,1)S(1)}, bf16[128,128]{1,0:T(8,128)(2,1)S(1)}, u32[]{:S(2)}, u32[]{:S(2)}) %collective-permute-start.12) | collective-permute-done | bytes 32800 | tf_op jit(solution)/shard_map/ppermute | solution.py:299
  11.8 3.7 %shard_map.118 = (bf16[128,256]{1,0:T(8,128)(2,1)}, bf16[128,256]{1,0:T(8,128)(2,1)}, bf16[128,256]{1,0:T(8,128)(2,1)}, bf16[128,256]{1,0:T(8,128)(2,1)}) custom-call(s32[1]{0:T(128)} %bitcast.1.me_ref, s32[1]{0:T(128)} %bitcast.2.first_ref, f32[4]{0:T(128)} %sink_ref.1, bf16[512,256]{1,0:T(8,128)(2,1)} %q_hbm.1, bf16[64,512]{1,0:T(8,128)(2,1)} %bitcast.24, ...), custom_call_target="tpu_custom_call" | custom-call | tf_op jit(solution)/shard_map/pallas_call | solution.py:323
  15.9 2.9 %collective-permute-start.14 = (bf16[128,256]{1,0:T(8,128)(2,1)}, bf16[128,256]{1,0:T(8,128)(2,1)S(1)}, u32[]{:S(2)}, u32[]{:S(2)}) collective-permute-start(bf16[128,256]{1,0:T(8,128)(2,1)} %get-tuple-element.28), channel_id=1, source_target_pairs={{0,2},{1,3},{2,0},{3,1},{4,6},{5,7},{6,4},{7,5},{8,10},{9,11},{10,... | collective-permute-start | bytes 196616 | tf_op jit(solution)/shard_map/ppermute | solution.py:21
  22.0 2.8 %collective-permute-start.2 = (bf16[128,1024]{1,0:T(8,128)(2,1)S(1)}, bf16[128,1024]{1,0:T(8,128)(2,1)S(1)}, u32[]{:S(2)}, u32[]{:S(2)}) collective-permute-start(bf16[128,1024]{1,0:T(8,128)(2,1)S(1)} %get-tuple-element.50), channel_id=1, source_target_pairs={{0,3},{1,0},{2,1},{3,2},{4,7},{5,4},{6,5},{7,6},{8,11},{9,8},{10,9... | collective-permute-start | bytes 786440 | tf_op jit(solution)/shard_map/ppermute | solution.py:21
  24.8 3.2 %collective-permute-start.5 = (bf16[128,1024]{1,0:T(8,128)(2,1)S(1)}, bf16[128,1024]{1,0:T(8,128)(2,1)S(1)}, u32[]{:S(2)}, u32[]{:S(2)}) collective-permute-start(bf16[128,1024]{1,0:T(8,128)(2,1)S(1)} %collective-permute-done.3.refs_3_), channel_id=1, source_target_pairs={{0,3},{1,0},{2,1},{3,2},{4,7},{5,4},{6,5},{7,6},{8,11},{9,8},{10,9... | collective-permute-start | bytes 786440 | tf_op jit(solution)/shard_map/ppermute | solution.py:21
  28.0 3.5 %collective-permute-done.1.refs_1_ = bf16[128,1024]{1,0:T(8,128)(2,1)S(1)} collective-permute-done((bf16[128,1024]{1,0:T(8,128)(2,1)S(1)}, bf16[128,1024]{1,0:T(8,128)(2,1)S(1)}, u32[]{:S(2)}, u32[]{:S(2)}) %collective-permute-start.1) | collective-permute-done | bytes 262176 | tf_op jit(solution)/shard_map/ppermute | solution.py:21
  32.0 2.4 %collective-permute-done.4.refs_4_ = bf16[128,1024]{1,0:T(8,128)(2,1)S(1)} collective-permute-done((bf16[128,1024]{1,0:T(8,128)(2,1)S(1)}, bf16[128,1024]{1,0:T(8,128)(2,1)S(1)}, u32[]{:S(2)}, u32[]{:S(2)}) %collective-permute-start.4) | collective-permute-done | bytes 262176 | tf_op jit(solution)/shard_map/ppermute | solution.py:21
  37.6 2.6 %shard_map.120 = (f32[128,2048]{1,0:T(8,128)S(1)}, bf16[512,1280]{1,0:T(8,128)(2,1)S(1)}) custom-call(s32[1]{0:T(128)} %bitcast.half_ref, bf16[128,1024]{1,0:T(8,128)(2,1)S(1)} %collective-permute-done.refs_0_, bf16[128,1024]{1,0:T(8,128)(2,1)S(1)} %collective-permute-done.1.refs_1_, bf16[128,1024]{1,0:T(8,128)(2,1)S(1)} %collective-permute-done.2.refs_2_, ...), custom_call_target="tpu_custom_call" | custom-call | tf_op jit(solution)/shard_map/pallas_call | solution.py:341
  40.2 46.3 %all_to_all.10 = bf16[64,8,1280]{2,1,0:T(8,128)(2,1)S(1)} all-to-all(bf16[64,8,1280]{2,1,0:T(8,128)(2,1)S(1)} %bitcast.19), channel_id=1, replica_groups=mesh['sp'=64,'tp'=4] {'sp'}, dimensions={0} | all-to-all | bytes 2621440 | tf_op jit(solution)/shard_map/all_to_all | solution.py:391
  87.5 2.5 %collective-permute-start.17 = (bf16[256,1280]{1,0:T(8,128)(2,1)S(1)}, bf16[256,1280]{1,0:T(8,128)(2,1)S(1)}, u32[]{:S(2)}, u32[]{:S(2)}) collective-permute-start(bf16[256,1280]{1,0:T(8,128)(2,1)S(1)} %get-tuple-element.47), channel_id=1, source_target_pairs={{0,3},{1,0},{2,1},{3,2},{4,7},{5,4},{6,5},{7,6},{8,11},{9,8},{10,9... | collective-permute-start | bytes 1966088 | tf_op jit(solution)/shard_map/ppermute | solution.py:21
  90.0 2.0 copy-done.8
  92.0 8.9 %shard_map.121 = (bf16[160,2048]{1,0:T(8,128)(2,1)S(1)}, bf16[160,2048]{1,0:T(8,128)(2,1)S(1)}) custom-call(bf16[512,1280]{1,0:T(8,128)(2,1)S(1)} %bitcast.17, bf16[1,2048,896]{2,1,0:T(8,128)(2,1)S(1)} %copy-done.6, bf16[1,2048,896]{2,1,0:T(8,128)(2,1)S(1)} %copy-done.7, bf16[1,896,2048]{2,1,0:T(8,128)(2,1)S(1)} %copy-done.8), custom_call_target="tpu_custom_call" | custom-call | flops 3523215360 | bytes 11010048 | tf_op jit(solution)/shard_map/pallas_call | solution.py:370
  100.9 2.1 collective-permute-done.16.refs_0_
  103.9 2.3 %collective-permute-start.23 = (bf16[256,1280]{1,0:T(8,128)(2,1)S(1)}, bf16[256,1280]{1,0:T(8,128)(2,1)S(1)}, u32[]{:S(2)}, u32[]{:S(2)}) collective-permute-start(bf16[256,1280]{1,0:T(8,128)(2,1)S(1)} %collective-permute-done.17.refs_3_), channel_id=1, source_target_pairs={{0,3},{1,0},{2,1},{3,2},{4,7},{5,4},{6,5},{7,6},{8,11},{9,8},{10,9... | collective-permute-start | bytes 1966088 | tf_op jit(solution)/shard_map/ppermute | solution.py:21
  106.3 3.2 %collective-permute-start.19 = (bf16[256,1280]{1,0:T(8,128)(2,1)S(1)}, bf16[256,1280]{1,0:T(8,128)(2,1)S(1)}, u32[]{:S(2)}, u32[]{:S(2)}) collective-permute-start(bf16[256,1280]{1,0:T(8,128)(2,1)S(1)} %get-tuple-element.48), channel_id=1, source_target_pairs={{0,3},{1,0},{2,1},{3,2},{4,7},{5,4},{6,5},{7,6},{8,11},{9,8},{10,9... | collective-permute-start | bytes 1966088 | tf_op jit(solution)/shard_map/ppermute | solution.py:21
  109.5 12.3 %collective-permute-done.22.refs_0_ = bf16[256,1280]{1,0:T(8,128)(2,1)S(1)} collective-permute-done((bf16[256,1280]{1,0:T(8,128)(2,1)S(1)}, bf16[256,1280]{1,0:T(8,128)(2,1)S(1)}, u32[]{:S(2)}, u32[]{:S(2)}) %collective-permute-start.22) | collective-permute-done | bytes 655392 | tf_op jit(solution)/shard_map/ppermute | solution.py:21
  121.9 8.9 %shard_map.123 = (bf16[160,2048]{1,0:T(8,128)(2,1)S(1)}, bf16[160,2048]{1,0:T(8,128)(2,1)S(1)}) custom-call(bf16[256,1280]{1,0:T(8,128)(2,1)S(1)} %collective-permute-done.22.refs_0_, bf16[256,1280]{1,0:T(8,128)(2,1)S(1)} %collective-permute-done.23.refs_1_, bf16[1,2048,896]{2,1,0:T(8,128)(2,1)S(1)} %copy-done.6, bf16[1,2048,896]{2,1,0:T(8,128)(2,1)S(1)} %copy-done.7, ...), custom_call_target="tpu_custom_call" | custom-call | flops 3523215360 | bytes 11010048 | tf_op jit(solution)/shard_map/pallas_call | solution.py:370
  135.9 13.4 %shard_map.122 = (bf16[160,2048]{1,0:T(8,128)(2,1)S(1)}, bf16[160,2048]{1,0:T(8,128)(2,1)S(1)}, bf16[160,2048]{1,0:T(8,128)(2,1)S(1)}, bf16[160,2048]{1,0:T(8,128)(2,1)S(1)}) custom-call(bf16[256,1280]{1,0:T(8,128)(2,1)S(1)} %collective-permute-done.16.refs_0_, bf16[256,1280]{1,0:T(8,128)(2,1)S(1)} %collective-permute-done.18.refs_1_, ...), custom_call_target="tpu_custom_call" | custom-call | flops 7046430720 | bytes 11010048 | tf_op jit(solution)/shard_map/pallas_call | solution.py:370
  153.3 3.2 %collective-permute-start.27 = (bf16[160,2048]{1,0:T(8,128)(2,1)S(1)}, bf16[160,2048]{1,0:T(8,128)(2,1)S(1)}, u32[]{:S(2)}, u32[]{:S(2)}) collective-permute-start(bf16[160,2048]{1,0:T(8,128)(2,1)S(1)} %add_convert_fusion), channel_id=1, source_target_pairs={{0,3},{1,0},{2,1},{3,2},{4,7},{5,4},{6,5},{7,6},{8,11},{9,8},{10,9... | collective-permute-start | bytes 1966088 | tf_op jit(solution)/shard_map/ppermute | solution.py:21
  156.5 11.2 %collective-permute-done.20.plus_ref = bf16[160,2048]{1,0:T(8,128)(2,1)S(1)} collective-permute-done((bf16[160,2048]{1,0:T(8,128)(2,1)S(1)}, bf16[160,2048]{1,0:T(8,128)(2,1)S(1)}, u32[]{:S(2)}, u32[]{:S(2)}) %collective-permute-start.20) | collective-permute-done | bytes 655392 | tf_op jit(solution)/shard_map/ppermute | solution.py:21
  167.7 7.0 %collective-permute-done.25.fromleft_ref = bf16[160,2048]{1,0:T(8,128)(2,1)S(1)} collective-permute-done((bf16[160,2048]{1,0:T(8,128)(2,1)S(1)}, bf16[160,2048]{1,0:T(8,128)(2,1)S(1)}, u32[]{:S(2)}, u32[]{:S(2)}) %collective-permute-start.25) | collective-permute-done | bytes 655392 | tf_op jit(solution)/shard_map/ppermute | solution.py:21
  175.9 44.9 %all_to_all.11 = bf16[64,8,1280]{2,1,0:T(8,128)(2,1)S(1)} all-to-all(bf16[64,8,1280]{2,1,0:T(8,128)(2,1)S(1)} %bitcast.16), channel_id=1, replica_groups=mesh['sp'=64,'tp'=4] {'sp'}, dimensions={0} | all-to-all | bytes 2621440 | tf_op jit(solution)/shard_map/all_to_all | solution.py:412
  220.7 2.7 %shard_map.125 = bf16[128,2048]{1,0:T(8,128)(2,1)} custom-call(bf16[512,1280]{1,0:T(8,128)(2,1)S(1)} %bitcast.18, bf16[320,128]{1,0:T(8,128)(2,1)S(1)} %get-tuple-element.43.refs_1_, bf16[320,128]{1,0:T(8,128)(2,1)S(1)} %get-tuple-element.44.refs_2_, f32[128,256]{1,0:T(8,128)S(1)} %get-tuple-element.45.refs_3_, f32[128,2048]{1,0:T(8,128)S(1)} %get-tuple-element.46.refs_4_), custom_call_target="tpu_custom_call" | custom-call | tf_op jit(solution)/shard_map/pallas_call | solution.py:415
  (69 shorter events, 25.9 us)
Async XLA Ops:
  1.2 23.6 %collective-permute-start = (bf16[128,1024]{1,0:T(8,128)(2,1)S(1)}, bf16[128,1024]{1,0:T(8,128)(2,1)S(1)}, u32[]{:S(2)}, u32[]{:S(2)}) collective-permute-start(bf16[128,1024]{1,0:T(8,128)(2,1)S(1)} %get-tuple-element.50), channel_id=1, source_target_pairs={{0,1},{1,2},{2,3},{3,0},{4,5},{5,6},{6,7},{7,4},{8,9},{9,10},{10,1... | collective-permute-start | bytes 786440 | tf_op jit(solution)/shard_map/ppermute | solution.py:21
  2.9 21.9 %collective-permute-start.3 = (bf16[128,1024]{1,0:T(8,128)(2,1)S(1)}, bf16[128,1024]{1,0:T(8,128)(2,1)S(1)}, u32[]{:S(2)}, u32[]{:S(2)}) collective-permute-start(bf16[128,1024]{1,0:T(8,128)(2,1)S(1)} %get-tuple-element.49), channel_id=1, source_target_pairs={{0,3},{1,0},{2,1},{3,2},{4,7},{5,4},{6,5},{7,6},{8,11},{9,8},{10,9... | collective-permute-start | bytes 786440 | tf_op jit(solution)/shard_map/ppermute | solution.py:21
  6.0 5.2 %collective-permute-start.12 = (bf16[128,128]{1,0:T(8,128)(2,1)S(1)}, bf16[128,128]{1,0:T(8,128)(2,1)S(1)}, u32[]{:S(2)}, u32[]{:S(2)}) collective-permute-start(bf16[128,128]{1,0:T(8,128)(2,1)S(1)} %pad_maximum_fusion), channel_id=1, source_target_pairs={{0,4},{4,8},{8,12},{12,16},{16,20},{20,24},{24,28},{28,32},{32,36}... | collective-permute-start | bytes 98312 | tf_op jit(solution)/shard_map/ppermute | solution.py:299
  15.5 5.8 %collective-permute-start.13 = (bf16[128,256]{1,0:T(8,128)(2,1)}, bf16[128,256]{1,0:T(8,128)(2,1)S(1)}, u32[]{:S(2)}, u32[]{:S(2)}) collective-permute-start(bf16[128,256]{1,0:T(8,128)(2,1)} %get-tuple-element.27), channel_id=1, source_target_pairs={{0,1},{1,2},{2,3},{3,0},{4,5},{5,6},{6,7},{7,4},{8,9},{9,10},{10,1... | collective-permute-start | bytes 196616 | tf_op jit(solution)/shard_map/ppermute | solution.py:21
  15.9 6.0 %collective-permute-start.14 = (bf16[128,256]{1,0:T(8,128)(2,1)}, bf16[128,256]{1,0:T(8,128)(2,1)S(1)}, u32[]{:S(2)}, u32[]{:S(2)}) collective-permute-start(bf16[128,256]{1,0:T(8,128)(2,1)} %get-tuple-element.28), channel_id=1, source_target_pairs={{0,2},{1,3},{2,0},{3,1},{4,6},{5,7},{6,4},{7,5},{8,10},{9,11},{10,... | collective-permute-start | bytes 196616 | tf_op jit(solution)/shard_map/ppermute | solution.py:21
  18.8 9.2 %collective-permute-start.15 = (bf16[128,256]{1,0:T(8,128)(2,1)}, bf16[128,256]{1,0:T(8,128)(2,1)S(1)}, u32[]{:S(2)}, u32[]{:S(2)}) collective-permute-start(bf16[128,256]{1,0:T(8,128)(2,1)} %get-tuple-element.29), channel_id=1, source_target_pairs={{0,3},{1,0},{2,1},{3,2},{4,7},{5,4},{6,5},{7,6},{8,11},{9,8},{10,9... | collective-permute-start | bytes 196616 | tf_op jit(solution)/shard_map/ppermute | solution.py:21
  21.3 10.2 %collective-permute-start.1 = (bf16[128,1024]{1,0:T(8,128)(2,1)S(1)}, bf16[128,1024]{1,0:T(8,128)(2,1)S(1)}, u32[]{:S(2)}, u32[]{:S(2)}) collective-permute-start(bf16[128,1024]{1,0:T(8,128)(2,1)S(1)} %get-tuple-element.49), channel_id=1, source_target_pairs={{0,1},{1,2},{2,3},{3,0},{4,5},{5,6},{6,7},{7,4},{8,9},{9,10},{10,1... | collective-permute-start | bytes 786440 | tf_op jit(solution)/shard_map/ppermute | solution.py:21
  22.0 9.5 %collective-permute-start.2 = (bf16[128,1024]{1,0:T(8,128)(2,1)S(1)}, bf16[128,1024]{1,0:T(8,128)(2,1)S(1)}, u32[]{:S(2)}, u32[]{:S(2)}) collective-permute-start(bf16[128,1024]{1,0:T(8,128)(2,1)S(1)} %get-tuple-element.50), channel_id=1, source_target_pairs={{0,3},{1,0},{2,1},{3,2},{4,7},{5,4},{6,5},{7,6},{8,11},{9,8},{10,9... | collective-permute-start | bytes 786440 | tf_op jit(solution)/shard_map/ppermute | solution.py:21
  24.8 9.7 %collective-permute-start.4 = (bf16[128,1024]{1,0:T(8,128)(2,1)S(1)}, bf16[128,1024]{1,0:T(8,128)(2,1)S(1)}, u32[]{:S(2)}, u32[]{:S(2)}) collective-permute-start(bf16[128,1024]{1,0:T(8,128)(2,1)S(1)} %collective-permute-done.refs_0_), channel_id=1, source_target_pairs={{0,1},{1,2},{2,3},{3,0},{4,5},{5,6},{6,7},{7,4},{8,9},{9,10},{10,1... | collective-permute-start | bytes 786440 | tf_op jit(solution)/shard_map/ppermute | solution.py:21
  24.8 9.7 %collective-permute-start.5 = (bf16[128,1024]{1,0:T(8,128)(2,1)S(1)}, bf16[128,1024]{1,0:T(8,128)(2,1)S(1)}, u32[]{:S(2)}, u32[]{:S(2)}) collective-permute-start(bf16[128,1024]{1,0:T(8,128)(2,1)S(1)} %collective-permute-done.3.refs_3_), channel_id=1, source_target_pairs={{0,3},{1,0},{2,1},{3,2},{4,7},{5,4},{6,5},{7,6},{8,11},{9,8},{10,9... | collective-permute-start | bytes 786440 | tf_op jit(solution)/shard_map/ppermute | solution.py:21
  28.0 6.9 %collective-permute-start.6 = (bf16[128,1024]{1,0:T(8,128)(2,1)S(1)}, bf16[128,1024]{1,0:T(8,128)(2,1)S(1)}, u32[]{:S(2)}, u32[]{:S(2)}) collective-permute-start(bf16[128,1024]{1,0:T(8,128)(2,1)S(1)} %collective-permute-done.refs_0_), channel_id=1, source_target_pairs={{0,4},{4,0},{8,12},{12,8},{16,20},{20,16},{24,28},{28,24},{32,36},... | collective-permute-start | bytes 786440 | tf_op jit(solution)/shard_map/ppermute | solution.py:26
  31.5 4.5 %collective-permute-start.9 = (bf16[128,1024]{1,0:T(8,128)(2,1)S(1)}, bf16[128,1024]{1,0:T(8,128)(2,1)S(1)}, u32[]{:S(2)}, u32[]{:S(2)}) collective-permute-start(bf16[128,1024]{1,0:T(8,128)(2,1)S(1)} %collective-permute-done.3.refs_3_), channel_id=1, source_target_pairs={{0,4},{4,0},{8,12},{12,8},{16,20},{20,16},{24,28},{28,24},{32,36},... | collective-permute-start | bytes 786440 | tf_op jit(solution)/shard_map/ppermute | solution.py:26
  86.6 16.4 %collective-permute-start.16 = (bf16[256,1280]{1,0:T(8,128)(2,1)S(1)}, bf16[256,1280]{1,0:T(8,128)(2,1)S(1)}, u32[]{:S(2)}, u32[]{:S(2)}) collective-permute-start(bf16[256,1280]{1,0:T(8,128)(2,1)S(1)} %get-tuple-element.48), channel_id=1, source_target_pairs={{0,1},{1,2},{2,3},{3,0},{4,5},{5,6},{6,7},{7,4},{8,9},{9,10},{10,1... | collective-permute-start | bytes 1966088 | tf_op jit(solution)/shard_map/ppermute | solution.py:21
  87.5 15.6 %collective-permute-start.17 = (bf16[256,1280]{1,0:T(8,128)(2,1)S(1)}, bf16[256,1280]{1,0:T(8,128)(2,1)S(1)}, u32[]{:S(2)}, u32[]{:S(2)}) collective-permute-start(bf16[256,1280]{1,0:T(8,128)(2,1)S(1)} %get-tuple-element.47), channel_id=1, source_target_pairs={{0,3},{1,0},{2,1},{3,2},{4,7},{5,4},{6,5},{7,6},{8,11},{9,8},{10,9... | collective-permute-start | bytes 1966088 | tf_op jit(solution)/shard_map/ppermute | solution.py:21
  103.0 18.8 %collective-permute-start.22 = (bf16[256,1280]{1,0:T(8,128)(2,1)S(1)}, bf16[256,1280]{1,0:T(8,128)(2,1)S(1)}, u32[]{:S(2)}, u32[]{:S(2)}) collective-permute-start(bf16[256,1280]{1,0:T(8,128)(2,1)S(1)} %collective-permute-done.16.refs_0_), channel_id=1, source_target_pairs={{0,1},{1,2},{2,3},{3,0},{4,5},{5,6},{6,7},{7,4},{8,9},{9,10},{10,1... | collective-permute-start | bytes 1966088 | tf_op jit(solution)/shard_map/ppermute | solution.py:21
  103.9 17.9 %collective-permute-start.23 = (bf16[256,1280]{1,0:T(8,128)(2,1)S(1)}, bf16[256,1280]{1,0:T(8,128)(2,1)S(1)}, u32[]{:S(2)}, u32[]{:S(2)}) collective-permute-start(bf16[256,1280]{1,0:T(8,128)(2,1)S(1)} %collective-permute-done.17.refs_3_), channel_id=1, source_target_pairs={{0,3},{1,0},{2,1},{3,2},{4,7},{5,4},{6,5},{7,6},{8,11},{9,8},{10,9... | collective-permute-start | bytes 1966088 | tf_op jit(solution)/shard_map/ppermute | solution.py:21
  106.3 29.6 %collective-permute-start.18 = (bf16[256,1280]{1,0:T(8,128)(2,1)S(1)}, bf16[256,1280]{1,0:T(8,128)(2,1)S(1)}, u32[]{:S(2)}, u32[]{:S(2)}) collective-permute-start(bf16[256,1280]{1,0:T(8,128)(2,1)S(1)} %get-tuple-element.47), channel_id=1, source_target_pairs={{0,1},{1,2},{2,3},{3,0},{4,5},{5,6},{6,7},{7,4},{8,9},{9,10},{10,1... | collective-permute-start | bytes 1966088 | tf_op jit(solution)/shard_map/ppermute | solution.py:21
  106.3 29.6 %collective-permute-start.19 = (bf16[256,1280]{1,0:T(8,128)(2,1)S(1)}, bf16[256,1280]{1,0:T(8,128)(2,1)S(1)}, u32[]{:S(2)}, u32[]{:S(2)}) collective-permute-start(bf16[256,1280]{1,0:T(8,128)(2,1)S(1)} %get-tuple-element.48), channel_id=1, source_target_pairs={{0,3},{1,0},{2,1},{3,2},{4,7},{5,4},{6,5},{7,6},{8,11},{9,8},{10,9... | collective-permute-start | bytes 1966088 | tf_op jit(solution)/shard_map/ppermute | solution.py:21
  130.7 21.9 %collective-permute-start.24 = (bf16[160,2048]{1,0:T(8,128)(2,1)S(1)}, bf16[160,2048]{1,0:T(8,128)(2,1)S(1)}, u32[]{:S(2)}, u32[]{:S(2)}) collective-permute-start(bf16[160,2048]{1,0:T(8,128)(2,1)S(1)} %get-tuple-element.40), channel_id=1, source_target_pairs={{0,1},{1,2},{2,3},{3,0},{4,5},{5,6},{6,7},{7,4},{8,9},{9,10},{10,1... | collective-permute-start | bytes 1966088 | tf_op jit(solution)/shard_map/ppermute | solution.py:21
  132.2 20.8 %collective-permute-start.26 = (bf16[160,2048]{1,0:T(8,128)(2,1)S(1)}, bf16[160,2048]{1,0:T(8,128)(2,1)S(1)}, u32[]{:S(2)}, u32[]{:S(2)}) collective-permute-start(bf16[160,2048]{1,0:T(8,128)(2,1)S(1)} %get-tuple-element.42), channel_id=1, source_target_pairs={{0,3},{1,0},{2,1},{3,2},{4,7},{5,4},{6,5},{7,6},{8,11},{9,8},{10,9... | collective-permute-start | bytes 1966088 | tf_op jit(solution)/shard_map/ppermute | solution.py:21
  149.3 18.4 %collective-permute-start.20 = (bf16[160,2048]{1,0:T(8,128)(2,1)S(1)}, bf16[160,2048]{1,0:T(8,128)(2,1)S(1)}, u32[]{:S(2)}, u32[]{:S(2)}) collective-permute-start(bf16[160,2048]{1,0:T(8,128)(2,1)S(1)} %get-tuple-element.37), channel_id=1, source_target_pairs={{0,1},{1,2},{2,3},{3,0},{4,5},{5,6},{6,7},{7,4},{8,9},{9,10},{10,1... | collective-permute-start | bytes 1966088 | tf_op jit(solution)/shard_map/ppermute | solution.py:21
  150.8 16.9 %collective-permute-start.21 = (bf16[160,2048]{1,0:T(8,128)(2,1)S(1)}, bf16[160,2048]{1,0:T(8,128)(2,1)S(1)}, u32[]{:S(2)}, u32[]{:S(2)}) collective-permute-start(bf16[160,2048]{1,0:T(8,128)(2,1)S(1)} %get-tuple-element.38), channel_id=1, source_target_pairs={{0,3},{1,0},{2,1},{3,2},{4,7},{5,4},{6,5},{7,6},{8,11},{9,8},{10,9... | collective-permute-start | bytes 1966088 | tf_op jit(solution)/shard_map/ppermute | solution.py:21
  152.9 21.8 %collective-permute-start.25 = (bf16[160,2048]{1,0:T(8,128)(2,1)S(1)}, bf16[160,2048]{1,0:T(8,128)(2,1)S(1)}, u32[]{:S(2)}, u32[]{:S(2)}) collective-permute-start(bf16[160,2048]{1,0:T(8,128)(2,1)S(1)} %add_convert_fusion.1), channel_id=1, source_target_pairs={{0,1},{1,2},{2,3},{3,0},{4,5},{5,6},{6,7},{7,4},{8,9},{9,10},{10,1... | collective-permute-start | bytes 1966088 | tf_op jit(solution)/shard_map/ppermute | solution.py:21
  153.3 21.4 %collective-permute-start.27 = (bf16[160,2048]{1,0:T(8,128)(2,1)S(1)}, bf16[160,2048]{1,0:T(8,128)(2,1)S(1)}, u32[]{:S(2)}, u32[]{:S(2)}) collective-permute-start(bf16[160,2048]{1,0:T(8,128)(2,1)S(1)} %add_convert_fusion), channel_id=1, source_target_pairs={{0,3},{1,0},{2,1},{3,2},{4,7},{5,4},{6,5},{7,6},{8,11},{9,8},{10,9... | collective-permute-start | bytes 1966088 | tf_op jit(solution)/shard_map/ppermute | solution.py:21
  (14 other events, 295.4 us)

commit v2 on v1

--- a/solution.py
+++ b/solution.py
@@ -16,9 +16,11 @@
 BF16 = jnp.bfloat16
 
 
-def around(value, by):
-    n = lax.axis_size("tp")
-    return lax.ppermute(value, "tp", [(i, (i + by) % n) for i in range(n)])
+EVEN, ACROSS, ODD = (1, 0, 3, 2), (2, 3, 0, 1), (3, 2, 1, 0)
+
+
+def exchange(value, peers):
+    return lax.ppermute(value, "tp", list(enumerate(peers)))
 
 
 def partner(value):
@@ -77,6 +79,22 @@
         wcol_ref[:, k * rows : (k + 1) * rows] = spread.T
 
 
+def split_body(half_ref, w_hbm, k_hbm, v_hbm, top_ref, bottom_ref, tail_ref, sems):
+    mid, wide = top_ref.shape
+    cols = pl.ds(pl.multiple_of(half_ref[0] * wide, wide), wide)
+    last = pl.ds(k_hbm.shape[1] - WINDOW, WINDOW)
+    copies = fetch_all(
+        (
+            (w_hbm.at[0:mid, cols], top_ref),
+            (w_hbm.at[mid : 2 * mid, cols], bottom_ref),
+            (k_hbm.at[:, last], tail_ref.at[0:DH, :]),
+            (v_hbm.at[:, last], tail_ref.at[DH : 2 * DH, :]),
+        ),
+        sems,
+    )
+    wait_all(copies)
+
+
 def attend_body(me_ref, first_ref, sink_ref, q_hbm, k_hbm, v_hbm, tail_ref, *refs):
     outs, (band_k, band_v, q_ref, k_ref, v_ref, sems) = refs[:4], refs[4:]
     copies = fetch_all(((q_hbm, q_ref), (k_hbm, k_ref), (v_hbm, v_ref)), sems)
@@ -92,7 +110,7 @@
     lower = lax.broadcasted_iota(jnp.int32, (2 * w, 1), 0) < w
     zero = jnp.zeros((DH, 2 * w), BF16)
     for i in range(4):
-        n = lax.rem(me_ref[0] + i, 4)
+        n = me_ref[0] ^ i
         at = pl.multiple_of(n * w, w)
         kb = band_k[0:DH, pl.ds(at, 2 * w)]
         vb = band_v[0:DH, pl.ds(at, 2 * w)]
@@ -143,13 +161,20 @@
 
 
 def project_body(cap, half_ref, *refs):
-    mine, theirs, (h0_ref, h1_ref, h2_ref, h3_ref), refs = refs[:6], refs[6:12], refs[12:16], refs[16:]
-    own_hbm, stream_hbm, gain_hbm, pick_hbm, mixed_hbm = refs[:5]
-    outs, (stage, own_ref, stream_ref, gain_ref, pick_ref, mixed_ref, sems) = refs[5:-7], refs[-7:]
+    mine, theirs, (h1_ref, h2_ref, h3_ref), refs = refs[:6], refs[6:12], refs[12:15], refs[15:]
+    h0_hbm, own_hbm, stream_hbm, gain_hbm, pick_hbm, mixed_hbm = refs[:6]
+    outs, (stage, h0_ref, own_ref, stream_ref, gain_ref, pick_ref, mixed_ref, sems) = refs[6:-8], refs[-8:]
     fetched = fetch_all(
-        ((own_hbm, own_ref), (stream_hbm, stream_ref), (gain_hbm, gain_ref), (pick_hbm, pick_ref)), sems
+        (
+            (h0_hbm, h0_ref),
+            (own_hbm, own_ref),
+            (stream_hbm, stream_ref),
+            (gain_hbm, gain_ref),
+            (pick_hbm, pick_ref),
+        ),
+        sems,
     )
-    h0, h1, h2, h3 = h0_ref[...], h1_ref[...], h2_ref[...], h3_ref[...]
+    h1, h2, h3 = h1_ref[...], h2_ref[...], h3_ref[...]
     mid = mine[0].shape[0]
     wide = own_ref.shape[1] // 2
     sides = [x for h in (h1, h3, h2) for x in (h[:, :mid], h[:, mid:])]
@@ -161,9 +186,9 @@
             part = one if part is None else part + one
         mixed_ref[:, here] = part
     wait_all(fetched)
-    mixed = mixed_ref[...] + dot(h0, own_ref[...]) + stream_ref[...].astype(F32)
+    mixed = mixed_ref[...] + dot(h0_ref[...], own_ref[...]) + stream_ref[...].astype(F32)
     mixed_ref[...] = mixed
-    kept = pltpu.make_async_copy(mixed_ref, mixed_hbm, sems.at[4])
+    kept = pltpu.make_async_copy(mixed_ref, mixed_hbm, sems.at[5])
     kept.start()
     scale = lax.rsqrt(jnp.mean(mixed * mixed, axis=1, keepdims=True) + EPSILON)
     normed = (mixed * scale * gain_ref[...]).astype(BF16)
@@ -277,10 +302,10 @@
             ).astype(BF16)
 
 
-def hop(up, down):
-    up = around(up, 1)
-    down = around(down, -1)
-    return up, down
+def hop(even, odd):
+    even = exchange(even, EVEN)
+    odd = exchange(odd, ODD)
+    return even, odd
 
 
 def on_device(queries, keys, values, sink_logits, stream, out_proj, norm_gain, routes, route_weights,
@@ -295,18 +320,22 @@
     sp, tp = lax.axis_index("sp"), lax.axis_index("tp")
     key_t, value_t = keys.T, values.T
 
-    tail = jnp.concatenate([key_t[:, tok_sp - WINDOW :], value_t[:, tok_sp - WINDOW :]], axis=0)
+    core = lax.rem(sp, 2)
+    mid, wide = width // 2, d // 2
+    w_top, w_bottom, tail = call(
+        split_body,
+        [jax.ShapeDtypeStruct((mid, wide), BF16)] * 2 + [jax.ShapeDtypeStruct((2 * DH, WINDOW), BF16)],
+        [pltpu.SemaphoreType.DMA((4,))],
+        in_specs=[smem] + [hbm] * 3,
+        out_specs=[vmem] * 3,
+        mib=58,
+    )(core.reshape(1), out_proj, key_t, value_t)
     tail = lax.ppermute(tail, "sp", [(i, i + 1) for i in range(experts - 1)])
 
-    core = lax.rem(sp, 2)
-    wide = d // 2
-    mid = width // 2
-    w_top = lax.dynamic_slice(out_proj, (0, core * wide), (mid, wide))
-    w_bottom = lax.dynamic_slice(out_proj, (mid, core * wide), (mid, wide))
-    left_top, right_bottom = hop(w_top, w_bottom)
-    left_bottom, right_top = hop(w_bottom, w_top)
-    far_top, far_bottom = hop(left_top, right_bottom)
-    gathered_w = [left_top, left_bottom, right_top, right_bottom, far_top, far_bottom]
+    even_top, odd_bottom = hop(w_top, w_bottom)
+    even_bottom, odd_top = hop(w_bottom, w_top)
+    far_bottom, far_top = hop(odd_bottom, even_top)
+    gathered_w = [even_top, even_bottom, odd_top, odd_bottom, far_top, far_bottom]
     for k in range(6):
         gathered_w.append(partner(gathered_w[k]))
 
@@ -336,7 +365,7 @@
     )(tp.reshape(1), (sp == 0).astype(jnp.int32).reshape(1), sink_logits, queries, key_t, value_t, tail)
     heads = list(heads)
     for i in (1, 2, 3):
-        heads[i] = around(heads[i], i)
+        heads[i] = exchange(heads[i], (EVEN, ACROSS, ODD)[i - 1])
 
     mixed, *outgoing = call(
         functools.partial(project_body, cap),
@@ -344,17 +373,18 @@
         + [jax.ShapeDtypeStruct((experts * 8, 256 * n), BF16) for n in CHUNKS],
         [
             pltpu.VMEM((2 * max(CHUNKS), experts * 8, 128), F32),
+            pltpu.VMEM((WINDOW, width), BF16),
             pltpu.VMEM((width, d), BF16),
             pltpu.VMEM((rows, d), BF16),
             pltpu.VMEM((1, d), F32),
             pltpu.VMEM((slots, rows), BF16),
             pltpu.VMEM((rows, d), F32),
-            pltpu.SemaphoreType.DMA((5,)),
+            pltpu.SemaphoreType.DMA((6,)),
         ],
-        in_specs=[smem] + [vmem] * 16 + [hbm] * 4,
+        in_specs=[smem] + [vmem] * 15 + [hbm] * 5,
         out_specs=[hbm] + [vmem] * len(CHUNKS),
         mib=20,
-    )(core.reshape(1), *gathered_w, *heads, out_proj, stream,
+    )(core.reshape(1), *gathered_w, *heads[1:], heads[0], out_proj, stream,
       norm_gain.reshape(1, d), pick)
 
     vm = lambda k: [vmem] * k
@@ -391,24 +421,23 @@
     arrived = lax.all_to_all(block, "sp", 0, 0, tiled=True).reshape(experts * 8, 256 * n)
     half = experts * 4
     top, bottom = arrived[:half], arrived[half:]
-    left_top, right_bottom = hop(top, bottom)
-    left_bottom, right_top = hop(bottom, top)
+    even_top, odd_bottom = hop(top, bottom)
+    even_bottom, odd_top = hop(bottom, top)
     own_top, own_bottom = run_experts(arrived)
-    left_top, right_bottom, own_top = tie((left_top, right_bottom, own_top))
-    far_a, far_b = hop(left_top, right_bottom)
-    p_top, p_bottom, m_top, m_bottom = run_experts(left_top, left_bottom, right_top, right_bottom)
-    plus = around(m_bottom, 1)
-    minus = around(p_top, -1)
-    y_a, y_b = run_experts(far_a, far_b)
-    top, bottom = add(m_top, around(y_a, 1)), add(p_bottom, around(y_b, -1))
-    from_left, from_right = around(top, 1), around(bottom, -1)
+    even_top, odd_bottom, own_top = tie((even_top, odd_bottom, own_top))
+    far_bottom, far_top = hop(odd_bottom, even_top)
+    e_top, e_bottom, o_top, o_bottom = run_experts(even_top, even_bottom, odd_top, odd_bottom)
+    plus, minus = hop(e_bottom, o_top)
+    y_top, y_bottom = run_experts(far_top, far_bottom)
+    y_bottom, y_top = hop(y_bottom, y_top)
+    from_even, from_odd = hop(add(e_top, y_top), add(o_bottom, y_bottom))
     back = call(
         functools.partial(gathered_body, n),
         jax.ShapeDtypeStruct((experts * 8, 256 * n), BF16),
         [pltpu.VMEM((2 * n, experts * 8, 128), F32)],
         in_specs=vm(6),
         out_specs=vmem,
-    )(own_top, own_bottom, plus, minus, from_left, from_right)
+    )(own_top, own_bottom, plus, minus, from_even, from_odd)
     back = lax.all_to_all(back.reshape(experts, 8, 256 * n), "sp", 0, 0, tiled=True)
     returned = [back.reshape(experts * 8, 256 * n)]
 

time: 224 us -> 226 us (level)
  waiting for transfers between devices: 46.8 us -> 56.8 us
  starting transfers between devices: 37.1 us -> 29.9 us
  local copies, waits for them, and re-layouts: 6.21 us -> 3.59 us
    ppermute x21, waiting for transfers between devices: 42.3 us -> 51.9 us  [exchange(): return lax.ppermute(value, 'tp', list(enumerate(peers)))]
    ppermute x21, starting transfers between devices: 34 us -> 27.4 us  [exchange(): return lax.ppermute(value, 'tp', list(enumerate(peers)))]
  transfers between devices with their start and end apart: 28 -> 28, of which waited for: 14 -> 16; matrix products, arithmetic and copies ran while one was open for 1% -> 0% of each run, Pallas kernels for 16% -> 16%
where the time goes in v2:
time: 226 us; the launch traced here: 225 us
  blocking collectives  90.7 us (40%)
  waiting for transfers between devices  56.8 us (25%)
  Pallas kernels  43.5 us (19%)
  starting transfers between devices  29.9 us (13%)
  local copies, waits for them, and re-layouts  3.59 us (2%)
    ppermute x21, waiting for transfers between devices, exchange(): return lax.ppermute(value, 'tp', list(enumerate(peers)))  51.9 us
    all_to_all x1, blocking collectives, on_device(): lax.all_to_all(block, 'sp', 0, 0, tiled=True).reshape(experts * 8, 256 * n)  45.9 us
    all_to_all x1, blocking collectives, on_device(): lax.all_to_all(back.reshape(experts, 8, 256 * n), 'sp', 0, 0, tiled=True)  44.9 us
    pallas_call x3, Pallas kernels, run_experts(): call(functools.partial(expert_body, n, len(blocks)), [jax.ShapeDtypeStruc...  31.1 us
    ppermute x21, starting transfers between devices, exchange(): return lax.ppermute(value, 'tp', list(enumerate(peers)))  27.4 us
  transfers between devices with their start and end apart: 28, of which 16 were waited for; matrix products, arithmetic and copies ran while one was open for 0% of the time, Pallas kernels for 16%

profile of v2, /device:TPU:2, one launch (start us, length us, event | category | flops | bytes accessed | tf_op | source)
XLA Modules:
  0.0 225.4 jit_solution(17120790804957662162)
XLA Ops:
  3.7 2.2 collective-permute-start.3
  7.8 3.5 %collective-permute-done.12.tail_ref = bf16[128,128]{1,0:T(8,128)(2,1)S(1)} collective-permute-done((bf16[128,128]{1,0:T(8,128)(2,1)}, bf16[128,128]{1,0:T(8,128)(2,1)S(1)}, u32[]{:S(2)}, u32[]{:S(2)}) %collective-permute-start.12) | collective-permute-done | bytes 32800 | tf_op jit(solution)/shard_map/ppermute | solution.py:333
  11.9 3.7 %shard_map.119 = (bf16[128,256]{1,0:T(8,128)(2,1)}, bf16[128,256]{1,0:T(8,128)(2,1)}, bf16[128,256]{1,0:T(8,128)(2,1)}, bf16[128,256]{1,0:T(8,128)(2,1)}) custom-call(s32[1]{0:T(128)} %bitcast.3.me_ref, s32[1]{0:T(128)} %bitcast.4.first_ref, f32[4]{0:T(128)} %sink_ref.1, bf16[512,256]{1,0:T(8,128)(2,1)} %q_hbm.1, bf16[64,512]{1,0:T(8,128)(2,1)} %bitcast.24, ...), custom_call_target="tpu_custom_call" | custom-call | tf_op jit(solution)/shard_map/pallas_call | solution.py:352
  18.2 2.2 collective-permute-start.15
  23.6 2.1 collective-permute-start.4
  26.4 2.2 collective-permute-done.1.refs_1_
  28.6 4.4 %collective-permute-done.2.refs_2_ = bf16[128,1024]{1,0:T(8,128)(2,1)S(1)} collective-permute-done((bf16[128,1024]{1,0:T(8,128)(2,1)}, bf16[128,1024]{1,0:T(8,128)(2,1)S(1)}, u32[]{:S(2)}, u32[]{:S(2)}) %collective-permute-start.2) | collective-permute-done | bytes 262176 | tf_op jit(solution)/shard_map/ppermute | solution.py:23
  33.0 3.0 %collective-permute-done.4.refs_4_ = bf16[128,1024]{1,0:T(8,128)(2,1)S(1)} collective-permute-done((bf16[128,1024]{1,0:T(8,128)(2,1)S(1)}, bf16[128,1024]{1,0:T(8,128)(2,1)S(1)}, u32[]{:S(2)}, u32[]{:S(2)}) %collective-permute-start.4) | collective-permute-done | bytes 262176 | tf_op jit(solution)/shard_map/ppermute | solution.py:23
  39.2 2.7 %shard_map.121 = (f32[128,2048]{1,0:T(8,128)S(1)}, bf16[512,1280]{1,0:T(8,128)(2,1)S(1)}) custom-call(s32[1]{0:T(128)} %bitcast.half_ref, bf16[128,1024]{1,0:T(8,128)(2,1)S(1)} %collective-permute-done.refs_0_, bf16[128,1024]{1,0:T(8,128)(2,1)S(1)} %collective-permute-done.1.refs_1_, bf16[128,1024]{1,0:T(8,128)(2,1)S(1)} %collective-permute-done.2.refs_2_, ...), custom_call_target="tpu_custom_call" | custom-call | tf_op jit(solution)/shard_map/pallas_call | solution.py:370
  41.9 45.9 %all_to_all.10 = bf16[64,8,1280]{2,1,0:T(8,128)(2,1)S(1)} all-to-all(bf16[64,8,1280]{2,1,0:T(8,128)(2,1)S(1)} %bitcast.19), channel_id=1, replica_groups=mesh['sp'=64,'tp'=4] {'sp'}, dimensions={0} | all-to-all | bytes 2621440 | tf_op jit(solution)/shard_map/all_to_all | solution.py:421
  88.0 2.0 collective-permute-start.17
  90.0 2.0 copy-done.8
  92.0 8.9 %shard_map.122 = (bf16[160,2048]{1,0:T(8,128)(2,1)S(1)}, bf16[160,2048]{1,0:T(8,128)(2,1)S(1)}) custom-call(bf16[512,1280]{1,0:T(8,128)(2,1)S(1)} %bitcast.17, bf16[1,2048,896]{2,1,0:T(8,128)(2,1)S(1)} %copy-done.6, bf16[1,2048,896]{2,1,0:T(8,128)(2,1)S(1)} %copy-done.7, bf16[1,896,2048]{2,1,0:T(8,128)(2,1)S(1)} %copy-done.8), custom_call_target="tpu_custom_call" | custom-call | flops 3523215360 | bytes 11010048 | tf_op jit(solution)/shard_map/pallas_call | solution.py:400
  100.9 2.1 collective-permute-done.16.refs_0_
  106.3 2.0 collective-permute-start.18
  109.7 13.5 %collective-permute-done.22.refs_0_ = bf16[256,1280]{1,0:T(8,128)(2,1)S(1)} collective-permute-done((bf16[256,1280]{1,0:T(8,128)(2,1)S(1)}, bf16[256,1280]{1,0:T(8,128)(2,1)S(1)}, u32[]{:S(2)}, u32[]{:S(2)}) %collective-permute-start.22) | collective-permute-done | bytes 655392 | tf_op jit(solution)/shard_map/ppermute | solution.py:23
  123.9 8.9 %shard_map.124 = (bf16[160,2048]{1,0:T(8,128)(2,1)S(1)}, bf16[160,2048]{1,0:T(8,128)(2,1)S(1)}) custom-call(bf16[256,1280]{1,0:T(8,128)(2,1)S(1)} %collective-permute-done.22.refs_0_, bf16[256,1280]{1,0:T(8,128)(2,1)S(1)} %collective-permute-done.23.refs_1_, bf16[1,2048,896]{2,1,0:T(8,128)(2,1)S(1)} %copy-done.6, bf16[1,2048,896]{2,1,0:T(8,128)(2,1)S(1)} %copy-done.7, ...), custom_call_target="tpu_custom_call" | custom-call | flops 3523215360 | bytes 11010048 | tf_op jit(solution)/shard_map/pallas_call | solution.py:400
  134.2 3.8 %collective-permute-done.18.refs_1_ = bf16[256,1280]{1,0:T(8,128)(2,1)S(1)} collective-permute-done((bf16[256,1280]{1,0:T(8,128)(2,1)S(1)}, bf16[256,1280]{1,0:T(8,128)(2,1)S(1)}, u32[]{:S(2)}, u32[]{:S(2)}) %collective-permute-start.18) | collective-permute-done | bytes 655392 | tf_op jit(solution)/shard_map/ppermute | solution.py:23
  138.0 13.3 %shard_map.123 = (bf16[160,2048]{1,0:T(8,128)(2,1)S(1)}, bf16[160,2048]{1,0:T(8,128)(2,1)S(1)}, bf16[160,2048]{1,0:T(8,128)(2,1)S(1)}, bf16[160,2048]{1,0:T(8,128)(2,1)S(1)}) custom-call(bf16[256,1280]{1,0:T(8,128)(2,1)S(1)} %collective-permute-done.16.refs_0_, bf16[256,1280]{1,0:T(8,128)(2,1)S(1)} %collective-permute-done.18.refs_1_, ...), custom_call_target="tpu_custom_call" | custom-call | flops 7046430720 | bytes 11010048 | tf_op jit(solution)/shard_map/pallas_call | solution.py:400
  154.7 2.0 collective-permute-start.27
  156.7 12.4 %collective-permute-done.20.plus_ref = bf16[160,2048]{1,0:T(8,128)(2,1)S(1)} collective-permute-done((bf16[160,2048]{1,0:T(8,128)(2,1)S(1)}, bf16[160,2048]{1,0:T(8,128)(2,1)S(1)}, u32[]{:S(2)}, u32[]{:S(2)}) %collective-permute-start.20) | collective-permute-done | bytes 655392 | tf_op jit(solution)/shard_map/ppermute | solution.py:23
  169.4 7.0 %collective-permute-done.25.fromleft_ref = bf16[160,2048]{1,0:T(8,128)(2,1)S(1)} collective-permute-done((bf16[160,2048]{1,0:T(8,128)(2,1)S(1)}, bf16[160,2048]{1,0:T(8,128)(2,1)S(1)}, u32[]{:S(2)}, u32[]{:S(2)}) %collective-permute-start.25) | collective-permute-done | bytes 655392 | tf_op jit(solution)/shard_map/ppermute | solution.py:23
  177.6 44.9 %all_to_all.11 = bf16[64,8,1280]{2,1,0:T(8,128)(2,1)S(1)} all-to-all(bf16[64,8,1280]{2,1,0:T(8,128)(2,1)S(1)} %bitcast.16), channel_id=1, replica_groups=mesh['sp'=64,'tp'=4] {'sp'}, dimensions={0} | all-to-all | bytes 2621440 | tf_op jit(solution)/shard_map/all_to_all | solution.py:441
  222.5 2.7 %shard_map.126 = bf16[128,2048]{1,0:T(8,128)(2,1)} custom-call(bf16[512,1280]{1,0:T(8,128)(2,1)S(1)} %bitcast.18, bf16[320,128]{1,0:T(8,128)(2,1)S(1)} %get-tuple-element.49.refs_1_, bf16[320,128]{1,0:T(8,128)(2,1)S(1)} %get-tuple-element.50.refs_2_, f32[128,256]{1,0:T(8,128)S(1)} %get-tuple-element.51.refs_3_, f32[128,2048]{1,0:T(8,128)S(1)} %get-tuple-element.52.refs_4_), custom_call_target="tpu_custom_call" | custom-call | tf_op jit(solution)/shard_map/pallas_call | solution.py:444
  (66 shorter events, 27.5 us)
Async XLA Ops:
  2.0 21.5 %collective-permute-start = (bf16[128,1024]{1,0:T(8,128)(2,1)}, bf16[128,1024]{1,0:T(8,128)(2,1)S(1)}, u32[]{:S(2)}, u32[]{:S(2)}) collective-permute-start(bf16[128,1024]{1,0:T(8,128)(2,1)} %get-tuple-element.29), channel_id=1, source_target_pairs={{0,1},{1,0},{2,3},{3,2},{4,5},{5,4},{6,7},{7,6},{8,9},{9,8},{10,11... | collective-permute-start | bytes 786440 | tf_op jit(solution)/shard_map/ppermute | solution.py:23
  3.7 22.0 %collective-permute-start.3 = (bf16[128,1024]{1,0:T(8,128)(2,1)}, bf16[128,1024]{1,0:T(8,128)(2,1)S(1)}, u32[]{:S(2)}, u32[]{:S(2)}) collective-permute-start(bf16[128,1024]{1,0:T(8,128)(2,1)} %get-tuple-element.30), channel_id=1, source_target_pairs={{0,3},{1,2},{2,1},{3,0},{4,7},{5,6},{6,5},{7,4},{8,11},{9,10},{10,... | collective-permute-start | bytes 786440 | tf_op jit(solution)/shard_map/ppermute | solution.py:23
  5.9 5.4 %collective-permute-start.12 = (bf16[128,128]{1,0:T(8,128)(2,1)}, bf16[128,128]{1,0:T(8,128)(2,1)S(1)}, u32[]{:S(2)}, u32[]{:S(2)}) collective-permute-start(bf16[128,128]{1,0:T(8,128)(2,1)} %get-tuple-element.31), channel_id=1, source_target_pairs={{0,4},{4,8},{8,12},{12,16},{16,20},{20,24},{24,28},{28,32},{32,36}... | collective-permute-start | bytes 98312 | tf_op jit(solution)/shard_map/ppermute | solution.py:333
  15.6 4.8 %collective-permute-start.13 = (bf16[128,256]{1,0:T(8,128)(2,1)}, bf16[128,256]{1,0:T(8,128)(2,1)S(1)}, u32[]{:S(2)}, u32[]{:S(2)}) collective-permute-start(bf16[128,256]{1,0:T(8,128)(2,1)} %get-tuple-element.32), channel_id=1, source_target_pairs={{0,1},{1,0},{2,3},{3,2},{4,5},{5,4},{6,7},{7,6},{8,9},{9,8},{10,11... | collective-permute-start | bytes 196616 | tf_op jit(solution)/shard_map/ppermute | solution.py:23
  16.3 6.1 %collective-permute-start.14 = (bf16[128,256]{1,0:T(8,128)(2,1)}, bf16[128,256]{1,0:T(8,128)(2,1)S(1)}, u32[]{:S(2)}, u32[]{:S(2)}) collective-permute-start(bf16[128,256]{1,0:T(8,128)(2,1)} %get-tuple-element.33), channel_id=1, source_target_pairs={{0,2},{1,3},{2,0},{3,1},{4,6},{5,7},{6,4},{7,5},{8,10},{9,11},{10,... | collective-permute-start | bytes 196616 | tf_op jit(solution)/shard_map/ppermute | solution.py:23
  18.2 8.2 %collective-permute-start.15 = (bf16[128,256]{1,0:T(8,128)(2,1)}, bf16[128,256]{1,0:T(8,128)(2,1)S(1)}, u32[]{:S(2)}, u32[]{:S(2)}) collective-permute-start(bf16[128,256]{1,0:T(8,128)(2,1)} %get-tuple-element.34), channel_id=1, source_target_pairs={{0,3},{1,2},{2,1},{3,0},{4,7},{5,6},{6,5},{7,4},{8,11},{9,10},{10,... | collective-permute-start | bytes 196616 | tf_op jit(solution)/shard_map/ppermute | solution.py:23
  20.4 8.2 %collective-permute-start.1 = (bf16[128,1024]{1,0:T(8,128)(2,1)}, bf16[128,1024]{1,0:T(8,128)(2,1)S(1)}, u32[]{:S(2)}, u32[]{:S(2)}) collective-permute-start(bf16[128,1024]{1,0:T(8,128)(2,1)} %get-tuple-element.30), channel_id=1, source_target_pairs={{0,1},{1,0},{2,3},{3,2},{4,5},{5,4},{6,7},{7,6},{8,9},{9,8},{10,11... | collective-permute-start | bytes 786440 | tf_op jit(solution)/shard_map/ppermute | solution.py:23
  22.4 10.6 %collective-permute-start.2 = (bf16[128,1024]{1,0:T(8,128)(2,1)}, bf16[128,1024]{1,0:T(8,128)(2,1)S(1)}, u32[]{:S(2)}, u32[]{:S(2)}) collective-permute-start(bf16[128,1024]{1,0:T(8,128)(2,1)} %get-tuple-element.29), channel_id=1, source_target_pairs={{0,3},{1,2},{2,1},{3,0},{4,7},{5,6},{6,5},{7,4},{8,11},{9,10},{10,... | collective-permute-start | bytes 786440 | tf_op jit(solution)/shard_map/ppermute | solution.py:23
  23.6 12.5 %collective-permute-start.4 = (bf16[128,1024]{1,0:T(8,128)(2,1)S(1)}, bf16[128,1024]{1,0:T(8,128)(2,1)S(1)}, u32[]{:S(2)}, u32[]{:S(2)}) collective-permute-start(bf16[128,1024]{1,0:T(8,128)(2,1)S(1)} %collective-permute-done.refs_0_), channel_id=1, source_target_pairs={{0,3},{1,2},{2,1},{3,0},{4,7},{5,6},{6,5},{7,4},{8,11},{9,10},{10,... | collective-permute-start | bytes 786440 | tf_op jit(solution)/shard_map/ppermute | solution.py:23
  25.7 10.4 %collective-permute-start.5 = (bf16[128,1024]{1,0:T(8,128)(2,1)S(1)}, bf16[128,1024]{1,0:T(8,128)(2,1)S(1)}, u32[]{:S(2)}, u32[]{:S(2)}) collective-permute-start(bf16[128,1024]{1,0:T(8,128)(2,1)S(1)} %collective-permute-done.3.refs_3_), channel_id=1, source_target_pairs={{0,1},{1,0},{2,3},{3,2},{4,5},{5,4},{6,7},{7,6},{8,9},{9,8},{10,11... | collective-permute-start | bytes 786440 | tf_op jit(solution)/shard_map/ppermute | solution.py:23
  26.4 10.2 %collective-permute-start.6 = (bf16[128,1024]{1,0:T(8,128)(2,1)S(1)}, bf16[128,1024]{1,0:T(8,128)(2,1)S(1)}, u32[]{:S(2)}, u32[]{:S(2)}) collective-permute-start(bf16[128,1024]{1,0:T(8,128)(2,1)S(1)} %collective-permute-done.refs_0_), channel_id=1, source_target_pairs={{0,4},{4,0},{8,12},{12,8},{16,20},{20,16},{24,28},{28,24},{32,36},... | collective-permute-start | bytes 786440 | tf_op jit(solution)/shard_map/ppermute | solution.py:28
  28.6 9.0 %collective-permute-start.9 = (bf16[128,1024]{1,0:T(8,128)(2,1)S(1)}, bf16[128,1024]{1,0:T(8,128)(2,1)S(1)}, u32[]{:S(2)}, u32[]{:S(2)}) collective-permute-start(bf16[128,1024]{1,0:T(8,128)(2,1)S(1)} %collective-permute-done.3.refs_3_), channel_id=1, source_target_pairs={{0,4},{4,0},{8,12},{12,8},{16,20},{20,16},{24,28},{28,24},{32,36},... | collective-permute-start | bytes 786440 | tf_op jit(solution)/shard_map/ppermute | solution.py:28
  87.9 15.2 %collective-permute-start.16 = (bf16[256,1280]{1,0:T(8,128)(2,1)S(1)}, bf16[256,1280]{1,0:T(8,128)(2,1)S(1)}, u32[]{:S(2)}, u32[]{:S(2)}) collective-permute-start(bf16[256,1280]{1,0:T(8,128)(2,1)S(1)} %get-tuple-element.54), channel_id=1, source_target_pairs={{0,1},{1,0},{2,3},{3,2},{4,5},{5,4},{6,7},{7,6},{8,9},{9,8},{10,11... | collective-permute-start | bytes 1966088 | tf_op jit(solution)/shard_map/ppermute | solution.py:23
  88.0 16.4 %collective-permute-start.17 = (bf16[256,1280]{1,0:T(8,128)(2,1)S(1)}, bf16[256,1280]{1,0:T(8,128)(2,1)S(1)}, u32[]{:S(2)}, u32[]{:S(2)}) collective-permute-start(bf16[256,1280]{1,0:T(8,128)(2,1)S(1)} %get-tuple-element.53), channel_id=1, source_target_pairs={{0,3},{1,2},{2,1},{3,0},{4,7},{5,6},{6,5},{7,4},{8,11},{9,10},{10,... | collective-permute-start | bytes 1966088 | tf_op jit(solution)/shard_map/ppermute | solution.py:23
  104.4 18.8 %collective-permute-start.22 = (bf16[256,1280]{1,0:T(8,128)(2,1)S(1)}, bf16[256,1280]{1,0:T(8,128)(2,1)S(1)}, u32[]{:S(2)}, u32[]{:S(2)}) collective-permute-start(bf16[256,1280]{1,0:T(8,128)(2,1)S(1)} %collective-permute-done.16.refs_0_), channel_id=1, source_target_pairs={{0,3},{1,2},{2,1},{3,0},{4,7},{5,6},{6,5},{7,4},{8,11},{9,10},{10,... | collective-permute-start | bytes 1966088 | tf_op jit(solution)/shard_map/ppermute | solution.py:23
  106.3 17.6 %collective-permute-start.23 = (bf16[256,1280]{1,0:T(8,128)(2,1)S(1)}, bf16[256,1280]{1,0:T(8,128)(2,1)S(1)}, u32[]{:S(2)}, u32[]{:S(2)}) collective-permute-start(bf16[256,1280]{1,0:T(8,128)(2,1)S(1)} %collective-permute-done.17.refs_3_), channel_id=1, source_target_pairs={{0,1},{1,0},{2,3},{3,2},{4,5},{5,4},{6,7},{7,6},{8,9},{9,8},{10,11... | collective-permute-start | bytes 1966088 | tf_op jit(solution)/shard_map/ppermute | solution.py:23
  106.3 31.6 %collective-permute-start.18 = (bf16[256,1280]{1,0:T(8,128)(2,1)S(1)}, bf16[256,1280]{1,0:T(8,128)(2,1)S(1)}, u32[]{:S(2)}, u32[]{:S(2)}) collective-permute-start(bf16[256,1280]{1,0:T(8,128)(2,1)S(1)} %get-tuple-element.53), channel_id=1, source_target_pairs={{0,1},{1,0},{2,3},{3,2},{4,5},{5,4},{6,7},{7,6},{8,9},{9,8},{10,11... | collective-permute-start | bytes 1966088 | tf_op jit(solution)/shard_map/ppermute | solution.py:23
  108.4 29.6 %collective-permute-start.19 = (bf16[256,1280]{1,0:T(8,128)(2,1)S(1)}, bf16[256,1280]{1,0:T(8,128)(2,1)S(1)}, u32[]{:S(2)}, u32[]{:S(2)}) collective-permute-start(bf16[256,1280]{1,0:T(8,128)(2,1)S(1)} %get-tuple-element.54), channel_id=1, source_target_pairs={{0,3},{1,2},{2,1},{3,0},{4,7},{5,6},{6,5},{7,4},{8,11},{9,10},{10,... | collective-permute-start | bytes 1966088 | tf_op jit(solution)/shard_map/ppermute | solution.py:23
  132.8 20.0 %collective-permute-start.24 = (bf16[160,2048]{1,0:T(8,128)(2,1)S(1)}, bf16[160,2048]{1,0:T(8,128)(2,1)S(1)}, u32[]{:S(2)}, u32[]{:S(2)}) collective-permute-start(bf16[160,2048]{1,0:T(8,128)(2,1)S(1)} %get-tuple-element.46), channel_id=1, source_target_pairs={{0,3},{1,2},{2,1},{3,0},{4,7},{5,6},{6,5},{7,4},{8,11},{9,10},{10,... | collective-permute-start | bytes 1966088 | tf_op jit(solution)/shard_map/ppermute | solution.py:23
  134.2 20.3 %collective-permute-start.26 = (bf16[160,2048]{1,0:T(8,128)(2,1)S(1)}, bf16[160,2048]{1,0:T(8,128)(2,1)S(1)}, u32[]{:S(2)}, u32[]{:S(2)}) collective-permute-start(bf16[160,2048]{1,0:T(8,128)(2,1)S(1)} %get-tuple-element.48), channel_id=1, source_target_pairs={{0,1},{1,0},{2,3},{3,2},{4,5},{5,4},{6,7},{7,6},{8,9},{9,8},{10,11... | collective-permute-start | bytes 1966088 | tf_op jit(solution)/shard_map/ppermute | solution.py:23
  151.3 17.7 %collective-permute-start.20 = (bf16[160,2048]{1,0:T(8,128)(2,1)S(1)}, bf16[160,2048]{1,0:T(8,128)(2,1)S(1)}, u32[]{:S(2)}, u32[]{:S(2)}) collective-permute-start(bf16[160,2048]{1,0:T(8,128)(2,1)S(1)} %get-tuple-element.43), channel_id=1, source_target_pairs={{0,1},{1,0},{2,3},{3,2},{4,5},{5,4},{6,7},{7,6},{8,9},{9,8},{10,11... | collective-permute-start | bytes 1966088 | tf_op jit(solution)/shard_map/ppermute | solution.py:23
  151.4 18.0 %collective-permute-start.21 = (bf16[160,2048]{1,0:T(8,128)(2,1)S(1)}, bf16[160,2048]{1,0:T(8,128)(2,1)S(1)}, u32[]{:S(2)}, u32[]{:S(2)}) collective-permute-start(bf16[160,2048]{1,0:T(8,128)(2,1)S(1)} %get-tuple-element.44), channel_id=1, source_target_pairs={{0,3},{1,2},{2,1},{3,0},{4,7},{5,6},{6,5},{7,4},{8,11},{9,10},{10,... | collective-permute-start | bytes 1966088 | tf_op jit(solution)/shard_map/ppermute | solution.py:23
  153.0 23.4 %collective-permute-start.25 = (bf16[160,2048]{1,0:T(8,128)(2,1)S(1)}, bf16[160,2048]{1,0:T(8,128)(2,1)S(1)}, u32[]{:S(2)}, u32[]{:S(2)}) collective-permute-start(bf16[160,2048]{1,0:T(8,128)(2,1)S(1)} %add_convert_fusion.1), channel_id=1, source_target_pairs={{0,1},{1,0},{2,3},{3,2},{4,5},{5,4},{6,7},{7,6},{8,9},{9,8},{10,11... | collective-permute-start | bytes 1966088 | tf_op jit(solution)/shard_map/ppermute | solution.py:23
  154.7 21.8 %collective-permute-start.27 = (bf16[160,2048]{1,0:T(8,128)(2,1)S(1)}, bf16[160,2048]{1,0:T(8,128)(2,1)S(1)}, u32[]{:S(2)}, u32[]{:S(2)}) collective-permute-start(bf16[160,2048]{1,0:T(8,128)(2,1)S(1)} %add_convert_fusion), channel_id=1, source_target_pairs={{0,3},{1,2},{2,1},{3,0},{4,7},{5,6},{6,5},{7,4},{8,11},{9,10},{10,... | collective-permute-start | bytes 1966088 | tf_op jit(solution)/shard_map/ppermute | solution.py:23
  (14 other events, 299.9 us)

commit v3 on v2

--- a/solution.py
+++ b/solution.py
@@ -54,7 +54,7 @@
         copy.wait()
 
 
-def route_body(cap, routes_hbm, w_hbm, pick_ref, pick0_ref, pick1_ref, wcol_ref, routes_ref, w_ref, sems):
+def route_body(cap, routes_hbm, w_hbm, pick_ref, across_ref, wcol_ref, routes_ref, w_ref, sems):
     wait_all(fetch_all(((routes_hbm, routes_ref), (w_hbm, w_ref)), sems))
     rows = routes_ref.shape[1]
     experts = pick_ref.shape[0] // cap
@@ -67,14 +67,16 @@
     hit1 = (ids == routes_ref[1:2, :]).astype(F32)
     rank0 = dot(hit0.astype(BF16), before)
     rank1 = dot(hit1.astype(BF16), before) + jnp.sum(hit0, axis=1, keepdims=True)
+    firsts, seconds = [], []
     for r in range(cap):
         at0 = jnp.where(rank0 == float(r), hit0, 0.0)
         at1 = jnp.where(rank1 == float(r), hit1, 0.0)
         here = slice(r * experts, (r + 1) * experts)
-        pick0_ref[here, :] = at0.astype(BF16)
-        pick1_ref[here, :] = at1.astype(BF16)
+        firsts.append(at0)
+        seconds.append(at1)
         pick_ref[here, :] = (at0 + at1).astype(BF16)
-    for k in range(2):
+    for k, parts in enumerate((firsts, seconds)):
+        across_ref[k * rows : (k + 1) * rows, :] = jnp.concatenate(parts, axis=0).T.astype(BF16)
         spread = jnp.broadcast_to(w_ref[k : k + 1, :], (rows, rows))
         wcol_ref[:, k * rows : (k + 1) * rows] = spread.T
 
@@ -274,12 +276,10 @@
 
 def combine_body(cap, *refs):
     rets, refs = refs[: len(CHUNKS)], refs[len(CHUNKS) :]
-    pick0_hbm, pick1_hbm, wcol_hbm, mixed_hbm, out_ref, stage, back = refs[:7]
-    pick0_ref, pick1_ref, wcol_ref, mixed_ref, sems = refs[7:]
-    fetched = fetch_all(
-        ((pick0_hbm, pick0_ref), (pick1_hbm, pick1_ref), (wcol_hbm, wcol_ref), (mixed_hbm, mixed_ref)), sems
-    )
-    experts = pick0_ref.shape[0] // cap
+    across_hbm, wcol_hbm, mixed_hbm, out_ref, stage, back = refs[:6]
+    across_ref, wcol_ref, mixed_ref, sems = refs[6:]
+    fetched = fetch_all(((across_hbm, across_ref), (wcol_hbm, wcol_ref), (mixed_hbm, mixed_ref)), sems)
+    experts = across_ref.shape[1] // cap
     slot = 0
     for ref, n in zip(rets, CHUNKS):
         load_stage(stage, ref, n)
@@ -288,11 +288,9 @@
             slot += 1
     wait_all(fetched)
     rows = mixed_ref.shape[0]
-    one = (((0,), (0,)), ((), ()))
     for t in range(mixed_ref.shape[1] // 256):
-        here = slice(t * 256, (t + 1) * 256)
-        o0 = lax.dot_general(pick0_ref[...], back[:, here], one, preferred_element_type=F32)
-        o1 = lax.dot_general(pick1_ref[...], back[:, here], one, preferred_element_type=F32)
+        both = dot(across_ref[...], back[:, t * 256 : (t + 1) * 256])
+        o0, o1 = both[:rows], both[rows:]
         for lane in range(0, 256, rows):
             at = slice(t * 256 + lane, t * 256 + lane + rows)
             out_ref[:, at] = (
@@ -340,12 +338,12 @@
         gathered_w.append(partner(gathered_w[k]))
 
     slots = experts * cap
-    pick, pick0, pick1, wcol = call(
+    pick, across, wcol = call(
         functools.partial(route_body, cap),
-        [jax.ShapeDtypeStruct((slots, rows), BF16)] * 3 + [jax.ShapeDtypeStruct((rows, 2 * rows), F32)],
+        [jax.ShapeDtypeStruct((slots, rows), BF16), jax.ShapeDtypeStruct((2 * rows, slots), BF16)] + [jax.ShapeDtypeStruct((rows, 2 * rows), F32)],
         [pltpu.VMEM((2, rows), jnp.int32), pltpu.VMEM((2, rows), F32), pltpu.SemaphoreType.DMA((2,))],
         in_specs=[hbm] * 2,
-        out_specs=[vmem] * 4,
+        out_specs=[vmem] * 3,
         mib=8,
     )(routes.T, route_weights.T)
 
@@ -447,16 +445,15 @@
         [
             pltpu.VMEM((2 * max(CHUNKS), experts * 8, 128), F32),
             pltpu.VMEM((slots, d), BF16),
-            pltpu.VMEM((slots, rows), BF16),
-            pltpu.VMEM((slots, rows), BF16),
+            pltpu.VMEM((2 * rows, slots), BF16),
             pltpu.VMEM((rows, 2 * rows), F32),
             pltpu.VMEM((rows, d), F32),
-            pltpu.SemaphoreType.DMA((4,)),
+            pltpu.SemaphoreType.DMA((3,)),
         ],
-        in_specs=vm(len(CHUNKS)) + [hbm] * 4,
+        in_specs=vm(len(CHUNKS)) + [hbm] * 3,
         out_specs=vmem,
         mib=20,
-    )(*returned, pick0, pick1, wcol, mixed)
+    )(*returned, across, wcol, mixed)
 
 
 def solution(mesh):

time: 226 us -> 226 us (level)
  no operation moved by 1% of the time
where the time goes in v3:
time: 226 us
  blocking collectives  90.9 us (40%)
  waiting for transfers between devices  56.7 us (25%)
  Pallas kernels  43.6 us (19%)
  starting transfers between devices  29.9 us (13%)
  local copies, waits for them, and re-layouts  3.59 us (2%)
    ppermute x21, waiting for transfers between devices, exchange(): return lax.ppermute(value, 'tp', list(enumerate(peers)))  51.9 us
    all_to_all x1, blocking collectives, on_device(): lax.all_to_all(block, 'sp', 0, 0, tiled=True).reshape(experts * 8, 256 * n)  46 us
    all_to_all x1, blocking collectives, on_device(): lax.all_to_all(back.reshape(experts, 8, 256 * n), 'sp', 0, 0, tiled=True)  44.9 us
    pallas_call x3, Pallas kernels, run_experts(): call(functools.partial(expert_body, n, len(blocks)), [jax.ShapeDtypeStruc...  31.1 us
    ppermute x21, starting transfers between devices, exchange(): return lax.ppermute(value, 'tp', list(enumerate(peers)))  27.4 us
  transfers between devices with their start and end apart: 28, of which 16 were waited for; matrix products, arithmetic and copies ran while one was open for 0% of the time, Pallas kernels for 16%

profile of v3, /device:TPU:2, one launch (start us, length us, event | category | flops | bytes accessed | tf_op | source)
XLA Modules:
  0.0 225.6 jit_solution(3193854903185538230)
XLA Ops:
  3.7 2.2 collective-permute-start.3
  7.8 3.5 %collective-permute-done.12.tail_ref = bf16[128,128]{1,0:T(8,128)(2,1)S(1)} collective-permute-done((bf16[128,128]{1,0:T(8,128)(2,1)}, bf16[128,128]{1,0:T(8,128)(2,1)S(1)}, u32[]{:S(2)}, u32[]{:S(2)}) %collective-permute-start.12) | collective-permute-done | bytes 32800 | tf_op jit(solution)/shard_map/ppermute | solution.py:331
  11.9 3.7 %shard_map.119 = (bf16[128,256]{1,0:T(8,128)(2,1)}, bf16[128,256]{1,0:T(8,128)(2,1)}, bf16[128,256]{1,0:T(8,128)(2,1)}, bf16[128,256]{1,0:T(8,128)(2,1)}) custom-call(s32[1]{0:T(128)} %bitcast.3.me_ref, s32[1]{0:T(128)} %bitcast.4.first_ref, f32[4]{0:T(128)} %sink_ref.1, bf16[512,256]{1,0:T(8,128)(2,1)} %q_hbm.1, bf16[64,512]{1,0:T(8,128)(2,1)} %bitcast.24, ...), custom_call_target="tpu_custom_call" | custom-call | tf_op jit(solution)/shard_map/pallas_call | solution.py:350
  18.2 2.2 collective-permute-start.15
  23.6 2.1 collective-permute-start.4
  26.4 2.2 collective-permute-done.1.refs_1_
  28.6 4.4 %collective-permute-done.2.refs_2_ = bf16[128,1024]{1,0:T(8,128)(2,1)S(1)} collective-permute-done((bf16[128,1024]{1,0:T(8,128)(2,1)}, bf16[128,1024]{1,0:T(8,128)(2,1)S(1)}, u32[]{:S(2)}, u32[]{:S(2)}) %collective-permute-start.2) | collective-permute-done | bytes 262176 | tf_op jit(solution)/shard_map/ppermute | solution.py:23
  33.0 3.0 %collective-permute-done.4.refs_4_ = bf16[128,1024]{1,0:T(8,128)(2,1)S(1)} collective-permute-done((bf16[128,1024]{1,0:T(8,128)(2,1)S(1)}, bf16[128,1024]{1,0:T(8,128)(2,1)S(1)}, u32[]{:S(2)}, u32[]{:S(2)}) %collective-permute-start.4) | collective-permute-done | bytes 262176 | tf_op jit(solution)/shard_map/ppermute | solution.py:23
  39.2 2.7 %shard_map.121 = (f32[128,2048]{1,0:T(8,128)S(1)}, bf16[512,1280]{1,0:T(8,128)(2,1)S(1)}) custom-call(s32[1]{0:T(128)} %bitcast.half_ref, bf16[128,1024]{1,0:T(8,128)(2,1)S(1)} %collective-permute-done.refs_0_, bf16[128,1024]{1,0:T(8,128)(2,1)S(1)} %collective-permute-done.1.refs_1_, bf16[128,1024]{1,0:T(8,128)(2,1)S(1)} %collective-permute-done.2.refs_2_, ...), custom_call_target="tpu_custom_call" | custom-call | tf_op jit(solution)/shard_map/pallas_call | solution.py:368
  41.9 46.0 %all_to_all.10 = bf16[64,8,1280]{2,1,0:T(8,128)(2,1)S(1)} all-to-all(bf16[64,8,1280]{2,1,0:T(8,128)(2,1)S(1)} %bitcast.19), channel_id=1, replica_groups=mesh['sp'=64,'tp'=4] {'sp'}, dimensions={0} | all-to-all | bytes 2621440 | tf_op jit(solution)/shard_map/all_to_all | solution.py:419
  88.2 2.0 collective-permute-start.17
  90.2 2.0 copy-done.8
  92.2 8.9 %shard_map.122 = (bf16[160,2048]{1,0:T(8,128)(2,1)S(1)}, bf16[160,2048]{1,0:T(8,128)(2,1)S(1)}) custom-call(bf16[512,1280]{1,0:T(8,128)(2,1)S(1)} %bitcast.18, bf16[1,2048,896]{2,1,0:T(8,128)(2,1)S(1)} %copy-done.6, bf16[1,2048,896]{2,1,0:T(8,128)(2,1)S(1)} %copy-done.7, bf16[1,896,2048]{2,1,0:T(8,128)(2,1)S(1)} %copy-done.8), custom_call_target="tpu_custom_call" | custom-call | flops 3523215360 | bytes 11010048 | tf_op jit(solution)/shard_map/pallas_call | solution.py:398
  101.1 2.1 collective-permute-done.16.refs_0_
  106.5 2.0 collective-permute-start.18
  109.8 13.5 %collective-permute-done.22.refs_0_ = bf16[256,1280]{1,0:T(8,128)(2,1)S(1)} collective-permute-done((bf16[256,1280]{1,0:T(8,128)(2,1)S(1)}, bf16[256,1280]{1,0:T(8,128)(2,1)S(1)}, u32[]{:S(2)}, u32[]{:S(2)}) %collective-permute-start.22) | collective-permute-done | bytes 655392 | tf_op jit(solution)/shard_map/ppermute | solution.py:23
  124.1 8.9 %shard_map.124 = (bf16[160,2048]{1,0:T(8,128)(2,1)S(1)}, bf16[160,2048]{1,0:T(8,128)(2,1)S(1)}) custom-call(bf16[256,1280]{1,0:T(8,128)(2,1)S(1)} %collective-permute-done.22.refs_0_, bf16[256,1280]{1,0:T(8,128)(2,1)S(1)} %collective-permute-done.23.refs_1_, bf16[1,2048,896]{2,1,0:T(8,128)(2,1)S(1)} %copy-done.6, bf16[1,2048,896]{2,1,0:T(8,128)(2,1)S(1)} %copy-done.7, ...), custom_call_target="tpu_custom_call" | custom-call | flops 3523215360 | bytes 11010048 | tf_op jit(solution)/shard_map/pallas_call | solution.py:398
  134.4 3.8 %collective-permute-done.18.refs_1_ = bf16[256,1280]{1,0:T(8,128)(2,1)S(1)} collective-permute-done((bf16[256,1280]{1,0:T(8,128)(2,1)S(1)}, bf16[256,1280]{1,0:T(8,128)(2,1)S(1)}, u32[]{:S(2)}, u32[]{:S(2)}) %collective-permute-start.18) | collective-permute-done | bytes 655392 | tf_op jit(solution)/shard_map/ppermute | solution.py:23
  138.2 13.4 %shard_map.123 = (bf16[160,2048]{1,0:T(8,128)(2,1)S(1)}, bf16[160,2048]{1,0:T(8,128)(2,1)S(1)}, bf16[160,2048]{1,0:T(8,128)(2,1)S(1)}, bf16[160,2048]{1,0:T(8,128)(2,1)S(1)}) custom-call(bf16[256,1280]{1,0:T(8,128)(2,1)S(1)} %collective-permute-done.16.refs_0_, bf16[256,1280]{1,0:T(8,128)(2,1)S(1)} %collective-permute-done.18.refs_1_, ...), custom_call_target="tpu_custom_call" | custom-call | flops 7046430720 | bytes 11010048 | tf_op jit(solution)/shard_map/pallas_call | solution.py:398
  154.8 2.0 collective-permute-start.27
  156.9 12.4 %collective-permute-done.20.plus_ref = bf16[160,2048]{1,0:T(8,128)(2,1)S(1)} collective-permute-done((bf16[160,2048]{1,0:T(8,128)(2,1)S(1)}, bf16[160,2048]{1,0:T(8,128)(2,1)S(1)}, u32[]{:S(2)}, u32[]{:S(2)}) %collective-permute-start.20) | collective-permute-done | bytes 655392 | tf_op jit(solution)/shard_map/ppermute | solution.py:23
  169.6 7.0 %collective-permute-done.25.fromleft_ref = bf16[160,2048]{1,0:T(8,128)(2,1)S(1)} collective-permute-done((bf16[160,2048]{1,0:T(8,128)(2,1)S(1)}, bf16[160,2048]{1,0:T(8,128)(2,1)S(1)}, u32[]{:S(2)}, u32[]{:S(2)}) %collective-permute-start.25) | collective-permute-done | bytes 655392 | tf_op jit(solution)/shard_map/ppermute | solution.py:23
  177.8 44.9 %all_to_all.11 = bf16[64,8,1280]{2,1,0:T(8,128)(2,1)S(1)} all-to-all(bf16[64,8,1280]{2,1,0:T(8,128)(2,1)S(1)} %bitcast.16), channel_id=1, replica_groups=mesh['sp'=64,'tp'=4] {'sp'}, dimensions={0} | all-to-all | bytes 2621440 | tf_op jit(solution)/shard_map/all_to_all | solution.py:439
  222.7 2.7 %shard_map.126 = bf16[128,2048]{1,0:T(8,128)(2,1)} custom-call(bf16[512,1280]{1,0:T(8,128)(2,1)S(1)} %bitcast.17, bf16[256,320]{1,0:T(8,128)(2,1)S(1)} %get-tuple-element.48.refs_1_, f32[128,256]{1,0:T(8,128)S(1)} %get-tuple-element.49.refs_2_, f32[128,2048]{1,0:T(8,128)S(1)} %get-tuple-element.50.refs_3_), custom_call_target="tpu_custom_call" | custom-call | tf_op jit(solution)/shard_map/pallas_call | solution.py:442
  (66 shorter events, 27.5 us)
Async XLA Ops:
  2.0 21.5 %collective-permute-start = (bf16[128,1024]{1,0:T(8,128)(2,1)}, bf16[128,1024]{1,0:T(8,128)(2,1)S(1)}, u32[]{:S(2)}, u32[]{:S(2)}) collective-permute-start(bf16[128,1024]{1,0:T(8,128)(2,1)} %get-tuple-element.28), channel_id=1, source_target_pairs={{0,1},{1,0},{2,3},{3,2},{4,5},{5,4},{6,7},{7,6},{8,9},{9,8},{10,11... | collective-permute-start | bytes 786440 | tf_op jit(solution)/shard_map/ppermute | solution.py:23
  3.7 22.0 %collective-permute-start.3 = (bf16[128,1024]{1,0:T(8,128)(2,1)}, bf16[128,1024]{1,0:T(8,128)(2,1)S(1)}, u32[]{:S(2)}, u32[]{:S(2)}) collective-permute-start(bf16[128,1024]{1,0:T(8,128)(2,1)} %get-tuple-element.29), channel_id=1, source_target_pairs={{0,3},{1,2},{2,1},{3,0},{4,7},{5,6},{6,5},{7,4},{8,11},{9,10},{10,... | collective-permute-start | bytes 786440 | tf_op jit(solution)/shard_map/ppermute | solution.py:23
  5.9 5.4 %collective-permute-start.12 = (bf16[128,128]{1,0:T(8,128)(2,1)}, bf16[128,128]{1,0:T(8,128)(2,1)S(1)}, u32[]{:S(2)}, u32[]{:S(2)}) collective-permute-start(bf16[128,128]{1,0:T(8,128)(2,1)} %get-tuple-element.30), channel_id=1, source_target_pairs={{0,4},{4,8},{8,12},{12,16},{16,20},{20,24},{24,28},{28,32},{32,36}... | collective-permute-start | bytes 98312 | tf_op jit(solution)/shard_map/ppermute | solution.py:331
  15.6 4.8 %collective-permute-start.13 = (bf16[128,256]{1,0:T(8,128)(2,1)}, bf16[128,256]{1,0:T(8,128)(2,1)S(1)}, u32[]{:S(2)}, u32[]{:S(2)}) collective-permute-start(bf16[128,256]{1,0:T(8,128)(2,1)} %get-tuple-element.31), channel_id=1, source_target_pairs={{0,1},{1,0},{2,3},{3,2},{4,5},{5,4},{6,7},{7,6},{8,9},{9,8},{10,11... | collective-permute-start | bytes 196616 | tf_op jit(solution)/shard_map/ppermute | solution.py:23
  16.3 6.1 %collective-permute-start.14 = (bf16[128,256]{1,0:T(8,128)(2,1)}, bf16[128,256]{1,0:T(8,128)(2,1)S(1)}, u32[]{:S(2)}, u32[]{:S(2)}) collective-permute-start(bf16[128,256]{1,0:T(8,128)(2,1)} %get-tuple-element.32), channel_id=1, source_target_pairs={{0,2},{1,3},{2,0},{3,1},{4,6},{5,7},{6,4},{7,5},{8,10},{9,11},{10,... | collective-permute-start | bytes 196616 | tf_op jit(solution)/shard_map/ppermute | solution.py:23
  18.2 8.2 %collective-permute-start.15 = (bf16[128,256]{1,0:T(8,128)(2,1)}, bf16[128,256]{1,0:T(8,128)(2,1)S(1)}, u32[]{:S(2)}, u32[]{:S(2)}) collective-permute-start(bf16[128,256]{1,0:T(8,128)(2,1)} %get-tuple-element.33), channel_id=1, source_target_pairs={{0,3},{1,2},{2,1},{3,0},{4,7},{5,6},{6,5},{7,4},{8,11},{9,10},{10,... | collective-permute-start | bytes 196616 | tf_op jit(solution)/shard_map/ppermute | solution.py:23
  20.4 8.2 %collective-permute-start.1 = (bf16[128,1024]{1,0:T(8,128)(2,1)}, bf16[128,1024]{1,0:T(8,128)(2,1)S(1)}, u32[]{:S(2)}, u32[]{:S(2)}) collective-permute-start(bf16[128,1024]{1,0:T(8,128)(2,1)} %get-tuple-element.29), channel_id=1, source_target_pairs={{0,1},{1,0},{2,3},{3,2},{4,5},{5,4},{6,7},{7,6},{8,9},{9,8},{10,11... | collective-permute-start | bytes 786440 | tf_op jit(solution)/shard_map/ppermute | solution.py:23
  22.4 10.6 %collective-permute-start.2 = (bf16[128,1024]{1,0:T(8,128)(2,1)}, bf16[128,1024]{1,0:T(8,128)(2,1)S(1)}, u32[]{:S(2)}, u32[]{:S(2)}) collective-permute-start(bf16[128,1024]{1,0:T(8,128)(2,1)} %get-tuple-element.28), channel_id=1, source_target_pairs={{0,3},{1,2},{2,1},{3,0},{4,7},{5,6},{6,5},{7,4},{8,11},{9,10},{10,... | collective-permute-start | bytes 786440 | tf_op jit(solution)/shard_map/ppermute | solution.py:23
  23.6 12.5 %collective-permute-start.4 = (bf16[128,1024]{1,0:T(8,128)(2,1)S(1)}, bf16[128,1024]{1,0:T(8,128)(2,1)S(1)}, u32[]{:S(2)}, u32[]{:S(2)}) collective-permute-start(bf16[128,1024]{1,0:T(8,128)(2,1)S(1)} %collective-permute-done.refs_0_), channel_id=1, source_target_pairs={{0,3},{1,2},{2,1},{3,0},{4,7},{5,6},{6,5},{7,4},{8,11},{9,10},{10,... | collective-permute-start | bytes 786440 | tf_op jit(solution)/shard_map/ppermute | solution.py:23
  25.7 10.4 %collective-permute-start.5 = (bf16[128,1024]{1,0:T(8,128)(2,1)S(1)}, bf16[128,1024]{1,0:T(8,128)(2,1)S(1)}, u32[]{:S(2)}, u32[]{:S(2)}) collective-permute-start(bf16[128,1024]{1,0:T(8,128)(2,1)S(1)} %collective-permute-done.3.refs_3_), channel_id=1, source_target_pairs={{0,1},{1,0},{2,3},{3,2},{4,5},{5,4},{6,7},{7,6},{8,9},{9,8},{10,11... | collective-permute-start | bytes 786440 | tf_op jit(solution)/shard_map/ppermute | solution.py:23
  26.4 10.2 %collective-permute-start.6 = (bf16[128,1024]{1,0:T(8,128)(2,1)S(1)}, bf16[128,1024]{1,0:T(8,128)(2,1)S(1)}, u32[]{:S(2)}, u32[]{:S(2)}) collective-permute-start(bf16[128,1024]{1,0:T(8,128)(2,1)S(1)} %collective-permute-done.refs_0_), channel_id=1, source_target_pairs={{0,4},{4,0},{8,12},{12,8},{16,20},{20,16},{24,28},{28,24},{32,36},... | collective-permute-start | bytes 786440 | tf_op jit(solution)/shard_map/ppermute | solution.py:28
  28.6 9.0 %collective-permute-start.9 = (bf16[128,1024]{1,0:T(8,128)(2,1)S(1)}, bf16[128,1024]{1,0:T(8,128)(2,1)S(1)}, u32[]{:S(2)}, u32[]{:S(2)}) collective-permute-start(bf16[128,1024]{1,0:T(8,128)(2,1)S(1)} %collective-permute-done.3.refs_3_), channel_id=1, source_target_pairs={{0,4},{4,0},{8,12},{12,8},{16,20},{20,16},{24,28},{28,24},{32,36},... | collective-permute-start | bytes 786440 | tf_op jit(solution)/shard_map/ppermute | solution.py:28
  88.1 15.2 %collective-permute-start.16 = (bf16[256,1280]{1,0:T(8,128)(2,1)S(1)}, bf16[256,1280]{1,0:T(8,128)(2,1)S(1)}, u32[]{:S(2)}, u32[]{:S(2)}) collective-permute-start(bf16[256,1280]{1,0:T(8,128)(2,1)S(1)} %get-tuple-element.52), channel_id=1, source_target_pairs={{0,1},{1,0},{2,3},{3,2},{4,5},{5,4},{6,7},{7,6},{8,9},{9,8},{10,11... | collective-permute-start | bytes 1966088 | tf_op jit(solution)/shard_map/ppermute | solution.py:23
  88.2 16.4 %collective-permute-start.17 = (bf16[256,1280]{1,0:T(8,128)(2,1)S(1)}, bf16[256,1280]{1,0:T(8,128)(2,1)S(1)}, u32[]{:S(2)}, u32[]{:S(2)}) collective-permute-start(bf16[256,1280]{1,0:T(8,128)(2,1)S(1)} %get-tuple-element.51), channel_id=1, source_target_pairs={{0,3},{1,2},{2,1},{3,0},{4,7},{5,6},{6,5},{7,4},{8,11},{9,10},{10,... | collective-permute-start | bytes 1966088 | tf_op jit(solution)/shard_map/ppermute | solution.py:23
  104.6 18.8 %collective-permute-start.22 = (bf16[256,1280]{1,0:T(8,128)(2,1)S(1)}, bf16[256,1280]{1,0:T(8,128)(2,1)S(1)}, u32[]{:S(2)}, u32[]{:S(2)}) collective-permute-start(bf16[256,1280]{1,0:T(8,128)(2,1)S(1)} %collective-permute-done.16.refs_0_), channel_id=1, source_target_pairs={{0,3},{1,2},{2,1},{3,0},{4,7},{5,6},{6,5},{7,4},{8,11},{9,10},{10,... | collective-permute-start | bytes 1966088 | tf_op jit(solution)/shard_map/ppermute | solution.py:23
  106.5 17.6 %collective-permute-start.23 = (bf16[256,1280]{1,0:T(8,128)(2,1)S(1)}, bf16[256,1280]{1,0:T(8,128)(2,1)S(1)}, u32[]{:S(2)}, u32[]{:S(2)}) collective-permute-start(bf16[256,1280]{1,0:T(8,128)(2,1)S(1)} %collective-permute-done.17.refs_3_), channel_id=1, source_target_pairs={{0,1},{1,0},{2,3},{3,2},{4,5},{5,4},{6,7},{7,6},{8,9},{9,8},{10,11... | collective-permute-start | bytes 1966088 | tf_op jit(solution)/shard_map/ppermute | solution.py:23
  106.5 31.6 %collective-permute-start.18 = (bf16[256,1280]{1,0:T(8,128)(2,1)S(1)}, bf16[256,1280]{1,0:T(8,128)(2,1)S(1)}, u32[]{:S(2)}, u32[]{:S(2)}) collective-permute-start(bf16[256,1280]{1,0:T(8,128)(2,1)S(1)} %get-tuple-element.51), channel_id=1, source_target_pairs={{0,1},{1,0},{2,3},{3,2},{4,5},{5,4},{6,7},{7,6},{8,9},{9,8},{10,11... | collective-permute-start | bytes 1966088 | tf_op jit(solution)/shard_map/ppermute | solution.py:23
  108.5 29.6 %collective-permute-start.19 = (bf16[256,1280]{1,0:T(8,128)(2,1)S(1)}, bf16[256,1280]{1,0:T(8,128)(2,1)S(1)}, u32[]{:S(2)}, u32[]{:S(2)}) collective-permute-start(bf16[256,1280]{1,0:T(8,128)(2,1)S(1)} %get-tuple-element.52), channel_id=1, source_target_pairs={{0,3},{1,2},{2,1},{3,0},{4,7},{5,6},{6,5},{7,4},{8,11},{9,10},{10,... | collective-permute-start | bytes 1966088 | tf_op jit(solution)/shard_map/ppermute | solution.py:23
  133.0 20.0 %collective-permute-start.24 = (bf16[160,2048]{1,0:T(8,128)(2,1)S(1)}, bf16[160,2048]{1,0:T(8,128)(2,1)S(1)}, u32[]{:S(2)}, u32[]{:S(2)}) collective-permute-start(bf16[160,2048]{1,0:T(8,128)(2,1)S(1)} %get-tuple-element.45), channel_id=1, source_target_pairs={{0,3},{1,2},{2,1},{3,0},{4,7},{5,6},{6,5},{7,4},{8,11},{9,10},{10,... | collective-permute-start | bytes 1966088 | tf_op jit(solution)/shard_map/ppermute | solution.py:23
  134.4 20.3 %collective-permute-start.26 = (bf16[160,2048]{1,0:T(8,128)(2,1)S(1)}, bf16[160,2048]{1,0:T(8,128)(2,1)S(1)}, u32[]{:S(2)}, u32[]{:S(2)}) collective-permute-start(bf16[160,2048]{1,0:T(8,128)(2,1)S(1)} %get-tuple-element.47), channel_id=1, source_target_pairs={{0,1},{1,0},{2,3},{3,2},{4,5},{5,4},{6,7},{7,6},{8,9},{9,8},{10,11... | collective-permute-start | bytes 1966088 | tf_op jit(solution)/shard_map/ppermute | solution.py:23
  151.5 17.7 %collective-permute-start.20 = (bf16[160,2048]{1,0:T(8,128)(2,1)S(1)}, bf16[160,2048]{1,0:T(8,128)(2,1)S(1)}, u32[]{:S(2)}, u32[]{:S(2)}) collective-permute-start(bf16[160,2048]{1,0:T(8,128)(2,1)S(1)} %get-tuple-element.42), channel_id=1, source_target_pairs={{0,1},{1,0},{2,3},{3,2},{4,5},{5,4},{6,7},{7,6},{8,9},{9,8},{10,11... | collective-permute-start | bytes 1966088 | tf_op jit(solution)/shard_map/ppermute | solution.py:23
  151.6 18.0 %collective-permute-start.21 = (bf16[160,2048]{1,0:T(8,128)(2,1)S(1)}, bf16[160,2048]{1,0:T(8,128)(2,1)S(1)}, u32[]{:S(2)}, u32[]{:S(2)}) collective-permute-start(bf16[160,2048]{1,0:T(8,128)(2,1)S(1)} %get-tuple-element.43), channel_id=1, source_target_pairs={{0,3},{1,2},{2,1},{3,0},{4,7},{5,6},{6,5},{7,4},{8,11},{9,10},{10,... | collective-permute-start | bytes 1966088 | tf_op jit(solution)/shard_map/ppermute | solution.py:23
  153.2 23.4 %collective-permute-start.25 = (bf16[160,2048]{1,0:T(8,128)(2,1)S(1)}, bf16[160,2048]{1,0:T(8,128)(2,1)S(1)}, u32[]{:S(2)}, u32[]{:S(2)}) collective-permute-start(bf16[160,2048]{1,0:T(8,128)(2,1)S(1)} %add_convert_fusion.1), channel_id=1, source_target_pairs={{0,1},{1,0},{2,3},{3,2},{4,5},{5,4},{6,7},{7,6},{8,9},{9,8},{10,11... | collective-permute-start | bytes 1966088 | tf_op jit(solution)/shard_map/ppermute | solution.py:23
  154.8 21.8 %collective-permute-start.27 = (bf16[160,2048]{1,0:T(8,128)(2,1)S(1)}, bf16[160,2048]{1,0:T(8,128)(2,1)S(1)}, u32[]{:S(2)}, u32[]{:S(2)}) collective-permute-start(bf16[160,2048]{1,0:T(8,128)(2,1)S(1)} %add_convert_fusion), channel_id=1, source_target_pairs={{0,3},{1,2},{2,1},{3,0},{4,7},{5,6},{6,5},{7,4},{8,11},{9,10},{10,... | collective-permute-start | bytes 1966088 | tf_op jit(solution)/shard_map/ppermute | solution.py:23
  (14 other events, 300.4 us)
